TPU v7x, 256 devices: a whole 4x4x8 slice. The times are simulated.
256 devices in a mesh: ep: 16 (over y, x), tp: 16 (over z, core).
Axes of the slice: x: 4, y: 4, z: 8, core: 2. Of those that a mesh axis runs over, the one named last changes fastest.
Arguments:
- receptance: bfloat16 [32768, 1024], P('ep', 'tp'), may hold values from -6 to 6
- key_in: bfloat16 [32768, 1024], P('ep', 'tp'), may hold values from -6 to 6
- payload_vectors: bfloat16 [32768, 1024], P('ep', 'tp'), may hold values from -6 to 6
- decay_in: bfloat16 [32768, 1024], P('ep', 'tp'), may hold values from -30 to 3
- rate_in: bfloat16 [32768, 1024], P('ep', 'tp'), may hold values from -30 to 6
- gate_in: bfloat16 [32768, 1024], P('ep', 'tp'), may hold values from -6 to 6
- norm_gain: float32 [1024], P('tp'), may hold values from 0.1 to 1.9
- out_weight: bfloat16 [1024, 2048], P('tp'), may hold values from -0.1875 to 0.1875
- moe_in: bfloat16 [32768, 2048], P(('ep', 'tp')), may hold values from -6 to 6
- moe_gain: float32 [2048], replicated, may hold values from 0.1 to 1.9
- routes: int32 [32768, 2], P(('ep', 'tp')), may hold values from 0 to 31, all different within a row; in each aligned block of 128 rows (0 to 127, 128 to 255, ...) at most 12 rows name the same one
- route_weights: float32 [32768, 2], P(('ep', 'tp')), may hold values from 0.2 to 1
- expert_gate: bfloat16 [32, 2048, 512], P('ep', None, 'tp'), may hold values from -0.125 to 0.125
- expert_up: bfloat16 [32, 2048, 512], P('ep', None, 'tp'), may hold values from -0.125 to 0.125
- expert_down: bfloat16 [32, 2048, 512], P('ep', None, 'tp'), may hold values from -0.25 to 0.25
- shared_gate: bfloat16 [2048, 512], replicated, may hold values from -0.125 to 0.125
- shared_up: bfloat16 [2048, 512], replicated, may hold values from -0.125 to 0.125
- shared_down: bfloat16 [512, 2048], replicated, may hold values from -0.25 to 0.25
Outputs:
- mixed: bfloat16 [32768, 2048], P(('ep', 'tp'))
- moe_out: bfloat16 [32768, 2048], P(('ep', 'tp'))
Inputs may be any that keep to these rules, and one draw needn't show every extreme that they name: `routes`: each token names 2 different experts; within the rows of one device no expert is named more than 12 times, a bound that some block reaches there.
All inputs are finite; a program needn't handle non-finite values.
Results may differ from a plain program's by a relative error of at most 0.019.
Values may be sent and summed in bfloat16 or wider, within the bound.
No kernel may reach another device: no remote copies, remote signals or barrier semaphores. Data moves between devices by JAX's collectives and lax.ppermute only.
A program may use at most 128 MiB of HBM per device.

v0:
```python
import jax
import jax.numpy as jnp
from jax import lax
from jax.experimental import pallas as pl
from jax.experimental.pallas import tpu as pltpu
from jax.sharding import Mesh
from jax.sharding import PartitionSpec as P

HEAD_DIM = 64
CHUNK = 128
GROUP = 4
SLOTS = 12
EP = ("ep_0", "ep_1")
EP_TP = ("ep_0", "ep_1", "tp")
BF = jnp.bfloat16
F32 = jnp.float32
VMEM_LIMIT = 56 * 1024 * 1024


def iota(shape, axis):
    return lax.broadcasted_iota(jnp.int32, shape, axis)


def mm(left, right):
    return jnp.dot(left.astype(BF), right.astype(BF), preferred_element_type=F32)


def mm3(left, right):
    left_high, right_high = left.astype(BF), right.astype(BF)
    left_low, right_low = left - left_high.astype(F32), right - right_high.astype(F32)
    return mm(left_high, right_high) + (mm(left_high, right_low) + mm(left_low, right_high))


def dot_dims(left, right, dims):
    return lax.dot_general(left, right, (dims, ((), ())), preferred_element_type=F32)


def scan_kernel(key_ref, recept_ref, value_ref, decay_ref, rate_ref, reads_ref, total_ref):
    dim, length = key_ref.shape
    n = CHUNK
    row, col = iota((n, n), 0), iota((n, n), 1)
    strict, inclusive = col < row, col <= row
    eye = (row == col).astype(F32)
    near = (row >> 4) == (col >> 4)
    bands = [
        ((row >> (k + 1)) == (col >> (k + 1))) & ((row >> k) != (col >> k)) for k in (4, 5, 6)
    ]
    left_half = col < dim
    upper = (row <= col).astype(BF)
    upper3 = jnp.concatenate([upper, upper, upper], axis=0)
    zero_dim = jnp.zeros((dim, n), F32)
    zero_pair = jnp.zeros((dim, 2 * n), BF)
    left_dim = iota((dim, n), 1) < dim

    def one_group(g, state):
        stage = []
        for j in range(GROUP):
            at = pl.ds(pl.multiple_of((g * GROUP + j) * n, n), n)
            keys = key_ref[:, at].astype(F32)
            recept = recept_ref[:, at].astype(F32)
            values = value_ref[:, at].astype(F32)
            unit = keys * lax.rsqrt(jnp.sum(keys * keys, axis=0, keepdims=True) + 1e-6)
            beta = unit * jax.nn.sigmoid(rate_ref[:, at].astype(F32))
            log_decay = jax.nn.sigmoid(decay_ref[:, at].astype(F32)) * (-0.6065306597126334)
            high = log_decay.astype(BF)
            rest = log_decay - high.astype(F32)
            mid = rest.astype(BF)
            low = (rest - mid.astype(F32)).astype(BF)
            cumul = jnp.dot(
                jnp.concatenate([high, mid, low], axis=1), upper3, preferred_element_type=F32
            )
            ending = cumul[:, n - 1 : n]
            grow = jnp.exp(-cumul)
            to_end = jnp.exp(ending - cumul)
            alpha_dec = -unit * jnp.exp(cumul - log_decay)
            query_dec = recept * jnp.exp(cumul)
            pair = jnp.concatenate([(beta * grow).astype(BF), (keys * grow).astype(BF)], axis=1)
            rows = jnp.concatenate([alpha_dec, query_dec], axis=0).T
            stage.append(
                dict(
                    rows=rows,
                    pair=jnp.concatenate(
                        [
                            jnp.concatenate([pair, zero_pair], axis=1),
                            jnp.concatenate([zero_pair, pair], axis=1),
                        ],
                        axis=0,
                    ),
                    value_rows=jnp.concatenate([zero_dim, values], axis=0).T,
                    beta_end=beta * to_end,
                    key_end=keys * to_end,
                    decay_all=jnp.exp(ending),
                )
            )
        for s in stage:
            scores = mm(s["rows"], s["pair"])
            s["couple"] = jnp.where(strict, scores[:, :n], 0.0)
            s["insert"] = jnp.where(strict, scores[:, n : 2 * n], 0.0)
            s["read_beta"] = jnp.where(inclusive, scores[:, 2 * n : 3 * n], 0.0)
            s["read_key"] = jnp.where(inclusive, scores[:, 3 * n :], 0.0)
        for s in stage:
            block = jnp.where(near, s["couple"], 0.0)
            s["inv"] = eye + block
            s["power"] = mm(block, block)
        for step in range(2):
            for s in stage:
                both = mm(jnp.concatenate([s["inv"], s["power"]], axis=0), s["power"])
                s["inv"] = s["inv"] + both[:n]
                s["power"] = both[n:]
        for s in stage:
            s["inv"] = s["inv"] + mm(s["inv"], s["power"])
        for band in bands:
            for s in stage:
                s["side"] = mm(jnp.where(band, s["couple"], 0.0), s["inv"])
            for s in stage:
                s["inv"] = s["inv"] + mm(s["inv"], s["side"])
        for s in stage:
            s["through"] = mm(jnp.concatenate([s["read_beta"], s["beta_end"]], axis=0), s["inv"])
        for s in stage:
            direct = jnp.concatenate([s["read_key"], s["key_end"]], axis=0)
            s["direct"] = mm(s["through"], s["insert"]) + direct
        for s in stage:
            sources = jnp.concatenate(
                [jnp.where(left_half, s["rows"], 0.0), s["value_rows"]], axis=0
            )
            maps = mm(jnp.concatenate([s["through"], s["direct"]], axis=1), sources)
            query = jnp.where(left_half, pltpu.roll(s["rows"], dim, 1), 0.0)
            s["reads"] = maps[:n] + query
            s["moves"] = maps[n:]
        for j, s in enumerate(stage):
            at = pl.ds(pl.multiple_of((g * GROUP + j) * n, n), n)
            left = jnp.concatenate([s["reads"], s["moves"]], axis=0)[:, :dim]
            met = mm(left, state)
            out = met[:n] + jnp.where(left_half, 0.0, s["reads"])
            reads_ref[:, at] = out.T
            state = s["decay_all"] * state + met[n:] + jnp.where(left_dim, 0.0, s["moves"])
        return state

    start = (iota((dim, n), 0) == iota((dim, n), 1)).astype(F32)
    total_ref[...] = lax.fori_loop(0, length // (n * GROUP), one_group, start)


def gate_kernel(here_ref, totals_ref, reads_ref, gate_ref, gain_ref, out_ref):
    dim = gate_ref.shape[0]
    right = iota((dim, 2 * dim), 1) >= dim

    def pass_device(d, entry):
        total = totals_ref[d]
        moved = mm3(total[:, :dim], entry)
        return jnp.where(right, moved + total, 0.0)

    entry = lax.fori_loop(0, here_ref[0], pass_device, jnp.zeros((dim, 2 * dim), F32))
    entry = jnp.concatenate([entry, jnp.zeros_like(entry)], axis=0).T[dim:, :dim]
    gain = jnp.broadcast_to(gain_ref[...], (dim, dim))
    same = iota((dim, dim), 0) == iota((dim, dim), 1)
    gain = jnp.sum(jnp.where(same, gain, 0.0), axis=1, keepdims=True)
    parts = out_ref.shape[0]
    n = out_ref.shape[2]
    step = 4

    for j in range(0, parts, step):
        at = slice(j * n, (j + step) * n)
        recur = mm(entry, reads_ref[:dim, at]) + reads_ref[dim:, at]
        centered = recur - jnp.mean(recur, axis=0, keepdims=True)
        spread = jnp.mean(centered * centered, axis=0, keepdims=True)
        normed = centered * lax.rsqrt(spread + 0.00064)
        gated = normed * gain * jax.nn.sigmoid(gate_ref[:, at].astype(F32))
        for k in range(step):
            out_ref[j + k] = gated[:, k * n : (k + 1) * n].astype(BF)


def slot_tables(routes, total, experts):
    tokens = routes.shape[1]
    expert = iota((experts, tokens), 0)
    first, second = routes[0:1] == expert, routes[1:2] == expert
    picked = first | second
    before = (iota((tokens, tokens), 0) < iota((tokens, tokens), 1)).astype(BF)
    rank = mm(picked.astype(F32), before)
    marked = jnp.where(picked, rank + 1.0, 0.0)

    def places(shape):
        r = iota(shape, 0)
        group = (r * 2731) >> 16
        q = r - group * 24
        odd = ((q >= 8) & (q < 16)) | (q >= 20)
        base = jnp.where(q < 8, 0, jnp.where(q < 16, 8, jnp.where(q < 20, 8, 12)))
        return group * 2 + odd.astype(jnp.int32), q - base

    owner, unused = places((total, experts))
    spread = (owner == iota((total, experts), 1)).astype(F32)
    unused, place = places((total, tokens))
    filled = mm(spread, marked) == (place + 1).astype(F32)
    return first, second, spread, filled


def dispatch_kernel(moe_ref, gain_ref, routes_ref, normed_ref, sent_ref):
    values = moe_ref[...].astype(F32)
    centered = values - jnp.mean(values, axis=1, keepdims=True)
    spread = jnp.mean(centered * centered, axis=1, keepdims=True)
    normed = (centered * lax.rsqrt(spread + 1e-05) * gain_ref[...]).astype(BF)
    normed_ref[...] = normed
    total = sent_ref.shape[0]
    filled = slot_tables(routes_ref[...], total, total // SLOTS)[3]
    sent_ref[...] = mm(filled.astype(F32), normed).astype(BF)


def expert_kernel(rows_ref, weights_ref, out_ref, sum_ref):
    e, half = pl.program_id(0), pl.program_id(1)
    groups, slots, width = rows_ref.shape
    rows = groups * 8
    hidden = weights_ref.shape[0] * weights_ref.shape[3]

    @pl.when((e == 0) & (half == 0))
    def _():
        sum_ref[...] = jnp.zeros_like(sum_ref)

    def go(which):
        own = rows_ref[:, 8 * which : 8 * which + 8].reshape(rows, width)
        shared = rows_ref[:, 16:24].reshape(rows, width)
        given = jnp.concatenate([own, shared], axis=0)
        gate = dot_dims(given, weights_ref[:, 0, 0].reshape(hidden, width), ((1,), (1,)))
        upper = dot_dims(given, weights_ref[:, 1, 0].reshape(hidden, width), ((1,), (1,)))
        act = gate * jax.nn.sigmoid(gate) * upper
        r = iota(act.shape, 0)
        mine = (r < rows) | (((r & 7) >= 4) == (which == 1))
        act = jnp.where(mine, act, 0.0).astype(BF)
        down = weights_ref[:, 2, 0].reshape(hidden, width)
        sum_ref[which * rows : (which + 1) * rows] += dot_dims(act[:rows], down, ((1,), (0,)))
        sum_ref[2 * rows :] += dot_dims(act[rows:], down, ((1,), (0,)))

    @pl.when(e == 0)
    def _():
        go(0)

    @pl.when(e == 1)
    def _():
        go(1)

    @pl.when((e == 1) & (half == 1))
    def _():
        for k in range(3):
            part = sum_ref[k * rows : (k + 1) * rows].reshape(groups, 8, width)
            out_ref[:, 8 * k : 8 * k + 8] = part.astype(BF)


def combine_kernel(routes_ref, weights_ref, results_ref, shared_ref, out_ref):
    total = results_ref.shape[0]
    first, second, spread, filled = slot_tables(routes_ref[...], total, total // SLOTS)
    weights = weights_ref[...]
    share = 2.5 * weights / jnp.sum(weights, axis=0, keepdims=True)
    chosen = jnp.where(first, share[0:1], 0.0) + jnp.where(second, share[1:2], 0.0)
    high = chosen.astype(BF).astype(F32)
    results = results_ref[...]
    out = shared_ref[...]
    for part in (high, chosen - high):
        taken = jnp.where(filled, mm(spread, part), 0.0)
        out = out + mm(taken.T, results)
    out_ref[...] = out.astype(BF)


def project_kernel(rows_ref, weight_ref, out_ref):
    out_ref[...] = dot_dims(rows_ref[...], weight_ref[...], ((0,), (0,))).astype(BF)


def call(kernel, out_shape, **options):
    return pl.pallas_call(
        kernel,
        out_shape=out_shape,
        name=kernel.__name__,
        compiler_params=pltpu.CompilerParams(vmem_limit_bytes=VMEM_LIMIT),
        **options,
    )


def shape(dims, dtype):
    return jax.ShapeDtypeStruct(dims, dtype)


def shards(
    receptance,
    key_in,
    payload_vectors,
    decay_in,
    rate_in,
    gate_in,
    norm_gain,
    out_weight,
    moe_in,
    moe_gain,
    routes,
    route_weights,
    expert_gate,
    expert_up,
    expert_down,
    shared_gate,
    shared_up,
    shared_down,
):
    groups, peers = lax.axis_size(EP), lax.axis_size("tp")
    here = lax.axis_index(EP)
    length, dim = key_in.shape
    tokens, width = moe_in.shape

    local_weights = jnp.stack([w.transpose(0, 2, 1) for w in (expert_gate, expert_up, expert_down)])
    all_weights = lax.all_gather(local_weights, "tp")
    out_weight, unused = lax.optimization_barrier((out_weight, local_weights))
    projection = lax.all_gather(out_weight, "tp", axis=0, tiled=True)

    slots = expert_gate.shape[0] * SLOTS
    normed, sent = call(
        dispatch_kernel,
        (shape((tokens, width), BF), shape((groups * slots, width), BF)),
    )(moe_in, moe_gain.reshape(1, width), routes.T)
    arrived = lax.all_to_all(
        sent.reshape(groups, slots, width), EP, split_axis=0, concat_axis=0, tiled=True
    )

    reads, total = call(
        scan_kernel, (shape((2 * dim, length), F32), shape((dim, 2 * dim), F32))
    )(key_in.T, receptance.T, payload_vectors.T, decay_in.T, rate_in.T)
    totals = lax.all_to_all(
        jnp.broadcast_to(total, (groups, dim, 2 * dim)),
        EP,
        split_axis=0,
        concat_axis=0,
        tiled=True,
    )
    smem = pl.BlockSpec(memory_space=pltpu.SMEM)
    vmem = pl.BlockSpec(memory_space=pltpu.VMEM)
    rows = call(
        gate_kernel,
        shape((peers, dim, length // peers), BF),
        in_specs=[smem] + [vmem] * 4,
    )(here.astype(jnp.int32).reshape(1), totals, reads, gate_in.T, norm_gain.reshape(1, dim))
    token_rows = lax.all_to_all(rows, "tp", split_axis=0, concat_axis=0, tiled=True)

    gate = jnp.dot(normed, shared_gate, preferred_element_type=F32)
    upper = jnp.dot(normed, shared_up, preferred_element_type=F32)
    hidden = (jax.nn.silu(gate) * upper).astype(BF)
    shared_term = jnp.dot(hidden, shared_down, preferred_element_type=F32)

    part = peers // 2
    units = expert_gate.shape[2]
    results = call(
        expert_kernel,
        shape((groups, slots, width), BF),
        grid=(2, 2),
        in_specs=[
            pl.BlockSpec((groups, slots, width), lambda e, h: (0, 0, 0)),
            pl.BlockSpec((part, 3, 1, units, width), lambda e, h: (h, 0, e, 0, 0)),
        ],
        out_specs=pl.BlockSpec((groups, slots, width), lambda e, h: (0, 0, 0)),
        scratch_shapes=[pltpu.VMEM((groups * slots, width), F32)],
    )(arrived, all_weights)
    returned = lax.all_to_all(results, EP, split_axis=0, concat_axis=0, tiled=True)
    moe_out = call(combine_kernel, shape((tokens, width), BF))(
        routes.T, route_weights.T, returned.reshape(groups * slots, width), shared_term
    )

    columns = width // 8
    mixed = call(
        project_kernel,
        shape((tokens, width), BF),
        grid=(width // columns,),
        in_specs=[
            pl.BlockSpec((peers * dim, tokens), lambda i: (0, 0)),
            pl.BlockSpec((peers * dim, columns), lambda i: (0, i)),
        ],
        out_specs=pl.BlockSpec((tokens, columns), lambda i: (0, i)),
    )(token_rows.reshape(peers * dim, tokens), projection)
    return (mixed, moe_out)


def solution(mesh):
    torus = Mesh(mesh.devices.reshape(4, 4, mesh.shape["tp"]), ("ep_0", "ep_1", "tp"))
    placed = (
        *(P(EP, "tp"),) * 6,
        P("tp"),
        P("tp", None),
        P(EP_TP, None),
        P(),
        P(EP_TP, None),
        P(EP_TP, None),
        *(P(EP, None, "tp"),) * 3,
        P(),
        P(),
        P(),
    )
    return jax.shard_map(
        shards,
        mesh=torus,
        in_specs=placed,
        out_specs=(P(EP_TP, None), P(EP_TP, None)),
        check_vma=False,
    )
```

profile of v0, /device:TPU:1, one launch (start us, length us, event | category | flops | bytes accessed | tf_op | source)
XLA Modules:
  0.0 155.0 jit_solution(4926844973400809821)
XLA Ops:
  7.2 0.0 copy-start
  7.2 0.0 all-gather.6.cloned.1.call-start
  7.2 2.2 %pad_maximum_fusion = bf16[3,2,32,2048]{3,2,1,0:T(8,128)(2,1)} fusion(bf16[1,2,32,2048]{3,2,1,0:T(8,128)(2,1)} %bitcast.37, bf16[1,2,32,2048]{3,2,1,0:T(8,128)(2,1)} %bitcast.38, bf16[1,2,32,2048]{3,2,1,0:T(8,128)(2,1)} %bitcast.39), kind=kLoop, calls=%fused_computation.3 | loop fusion | flops 786432 | bytes 1572864 | tf_op jit(solution)/shard_map/stack | solution.py:304
  9.5 0.0 all-gather.6.cloned.1.call-update
  9.5 0.0 all-gather.4.cloned.1.call-start
  9.5 0.7 all-gather.4.cloned.1.call-update
  10.2 14.2 %scan_kernel.1 = (f32[128,2048]{1,0:T(8,128)}, f32[64,128]{1,0:T(8,128)}) custom-call(bf16[64,2048]{1,0:T(8,128)(2,1)} %bitcast.32, bf16[64,2048]{1,0:T(8,128)(2,1)} %bitcast.33, bf16[64,2048]{1,0:T(8,128)(2,1)} %bitcast.34, bf16[64,2048]{1,0:T(8,128)(2,1)} %bitcast.35, bf16[64,2048]{1,0:T(8,128)(2,1)} %bitcast.36), custom_call_target="tpu_custom_call" | custom-call | tf_op jit(solution)/shard_map/scan_kernel/pallas_call | solution.py:318
  24.4 1.6 %broadcast_in_dim.3 = f32[16,64,128]{2,1,0:T(8,128)} broadcast(f32[64,128]{1,0:T(8,128)} %get-tuple-element.7), dimensions={1,2} | broadcast | bytes 557056 | tf_op jit(solution)/shard_map/broadcast_in_dim | solution.py:322
  26.0 7.6 %all-to-all-start = ((f32[16,64,128]{2,1,0:T(8,128)}), f32[16,64,128]{2,1,0:T(8,128)S(1)}, u32[]{:S(2)}, u32[]{:S(2)}) async-start(f32[16,64,128]{2,1,0:T(8,128)} %broadcast_in_dim.3), calls=%async_computation | async-start | bytes 1048576 | tf_op jit(solution)/shard_map/all_to_all | solution.py:321
  33.6 3.2 %dispatch_kernel.1 = (bf16[128,2048]{1,0:T(8,128)(2,1)}, bf16[384,2048]{1,0:T(8,128)(2,1)}) custom-call(bf16[128,2048]{1,0:T(8,128)(2,1)} %moe_ref.1, f32[1,2048]{1,0:T(1,128)} %bitcast.41, s32[2,128]{1,0:T(2,128)} %bitcast.42), custom_call_target="tpu_custom_call" | custom-call | tf_op jit(solution)/shard_map/dispatch_kernel/pallas_call | solution.py:310
  36.8 7.2 %all-to-all-done.totals_ref = f32[16,64,128]{2,1,0:T(8,128)S(1)} async-done(((f32[16,64,128]{2,1,0:T(8,128)}), f32[16,64,128]{2,1,0:T(8,128)S(1)}, u32[]{:S(2)}, u32[]{:S(2)}) %all-to-all-start) | async-done | bytes 524320 | tf_op jit(solution)/shard_map/all_to_all | solution.py:321
  44.0 0.0 copy-start.2
  44.0 4.4 %all-to-all-start.2 = ((bf16[16,24,2048]{2,1,0:T(8,128)(2,1)}), bf16[16,24,2048]{2,1,0:T(8,128)(2,1)}, u32[]{:S(2)}, u32[]{:S(2)}) async-start(bf16[16,24,2048]{2,1,0:T(8,128)(2,1)} %bitcast.30), calls=%async_computation.2 | async-start | bytes 3145728 | tf_op jit(solution)/shard_map/all_to_all | solution.py:314
  48.4 0.0 copy-done.2
  48.4 2.6 %gate_kernel.1 = bf16[16,64,128]{2,1,0:T(8,128)(2,1)} custom-call(s32[1]{0:T(128)} %bitcast.here_ref, f32[16,64,128]{2,1,0:T(8,128)} %copy-done.2, f32[128,2048]{1,0:T(8,128)} %get-tuple-element.8.reads_ref, bf16[64,2048]{1,0:T(8,128)(2,1)} %bitcast.40, f32[1,64]{1,0:T(1,128)} %bitcast.45), custom_call_target="tpu_custom_call" | custom-call | tf_op jit(solution)/shard_map/gate_kernel/pallas_call | solution.py:330
  51.1 17.9 %all-to-all-done.2.rows_ref = bf16[16,24,2048]{2,1,0:T(8,128)(2,1)} async-done(((bf16[16,24,2048]{2,1,0:T(8,128)(2,1)}), bf16[16,24,2048]{2,1,0:T(8,128)(2,1)}, u32[]{:S(2)}, u32[]{:S(2)}) %all-to-all-start.2) | async-done | bytes 1572896 | tf_op jit(solution)/shard_map/all_to_all | solution.py:314
  69.0 12.4 %all-to-all-start.1 = ((bf16[16,64,128]{2,1,0:T(8,128)(2,1)}), bf16[16,64,128]{2,1,0:T(8,128)(2,1)S(1)}, u32[]{:S(2)}, u32[]{:S(2)}) async-start(bf16[16,64,128]{2,1,0:T(8,128)(2,1)} %gate_kernel.1), calls=%async_computation.1 | async-start | bytes 524288 | tf_op jit(solution)/shard_map/all_to_all | solution.py:335
  81.4 12.9 %all-gather.6.cloned.1.call-done = bf16[48,2,32,2048]{3,2,1,0:T(8,128)(2,1)} async-done(((bf16[3,2,32,2048]{3,2,1,0:T(8,128)(2,1)}), bf16[48,2,32,2048]{3,2,1,0:T(8,128)(2,1)}) %all-gather.6.cloned.1.call-update) | async-done | bytes 12582928 | tf_op jit(solution)/shard_map/all_gather | solution.py:305
  94.4 9.3 %expert_kernel.1 = bf16[16,24,2048]{2,1,0:T(8,128)(2,1)} custom-call(bf16[16,24,2048]{2,1,0:T(8,128)(2,1)} %all-to-all-done.2.rows_ref, bf16[16,3,2,32,2048]{4,3,2,1,0:T(8,128)(2,1)} %bitcast.29), custom_call_target="tpu_custom_call" | custom-call | tf_op jit(solution)/shard_map/expert_kernel/pallas_call | solution.py:344
  103.7 0.0 copy-start.1
  103.7 0.0 all-to-all-done.1
  103.7 0.0 copy-start.3
  103.7 7.6 %all-to-all-start.3 = ((bf16[16,24,2048]{2,1,0:T(8,128)(2,1)}), bf16[16,24,2048]{2,1,0:T(8,128)(2,1)}, u32[]{:S(2)}, u32[]{:S(2)}) async-start(bf16[16,24,2048]{2,1,0:T(8,128)(2,1)} %expert_kernel.1), calls=%async_computation.3 | async-start | bytes 3145728 | tf_op jit(solution)/shard_map/all_to_all | solution.py:355
  111.3 0.0 copy-done.1
  111.3 2.1 %fusion.9 = f32[128,512]{1,0:T(8,128)S(1)} fusion(bf16[128,2048]{1,0:T(8,128)(2,1)S(1)} %copy-done.1, bf16[2048,512]{1,0:T(8,128)(2,1)} %param.33), kind=kOutput, calls=%fused_computation.11 | convolution fusion | flops 268435456 | bytes 2883584 | tf_op jit(solution)/shard_map/dot_general | solution.py:337
  113.4 0.0 copy-done.3
  113.4 0.0 copy-done
  113.4 3.5 %fusion.1.shared_ref = f32[128,2048]{1,0:T(8,128)} fusion(bf16[512,2048]{1,0:T(8,128)(2,1)S(1)} %copy-done, bf16[128,2048]{1,0:T(8,128)(2,1)S(1)} %copy-done.1, bf16[2048,512]{1,0:T(8,128)(2,1)} %param.34, f32[128,512]{1,0:T(8,128)S(1)} %fusion.9), kind=kOutput, calls=%fused_computation.2 | convolution fusion | flops 537264128 | bytes 6029312 | tf_op jit(solution)/shard_map/dot_general | solution.py:340
  116.9 20.6 %all-gather.4.cloned.1.call-done.weight_ref = bf16[1024,2048]{1,0:T(8,128)(2,1)} async-done(((bf16[64,2048]{1,0:T(8,128)(2,1)}), bf16[1024,2048]{1,0:T(8,128)(2,1)}) %all-gather.4.cloned.1.call-update) | async-done | bytes 4194320 | tf_op jit(solution)/shard_map/all_gather | solution.py:307
  137.5 6.8 %project_kernel.1 = bf16[128,2048]{1,0:T(8,128)(2,1)} custom-call(bf16[1024,128]{1,0:T(8,128)(2,1)} %bitcast.31, bf16[1024,2048]{1,0:T(8,128)(2,1)} %all-gather.4.cloned.1.call-done.weight_ref), custom_call_target="tpu_custom_call" | custom-call | tf_op jit(solution)/shard_map/project_kernel/pallas_call | solution.py:361
  144.3 0.0 all-to-all-done.3
  144.3 3.8 %combine_kernel.1 = bf16[128,2048]{1,0:T(8,128)(2,1)} custom-call(s32[2,128]{1,0:T(2,128)} %bitcast.43, f32[2,128]{1,0:T(2,128)} %bitcast.44, bf16[384,2048]{1,0:T(8,128)(2,1)} %bitcast.20.results_ref, f32[128,2048]{1,0:T(8,128)} %fusion.1.shared_ref), custom_call_target="tpu_custom_call" | custom-call | tf_op jit(solution)/shard_map/combine_kernel/pallas_call | solution.py:356
Async XLA Ops:
  7.2 106.3 %copy-start = (bf16[512,2048]{1,0:T(8,128)(2,1)S(1)}, bf16[512,2048]{1,0:T(8,128)(2,1)}, u32[]{:S(2)}) copy-start(bf16[512,2048]{1,0:T(8,128)(2,1)} %param.35) | copy-start | bytes 6291460
  7.2 87.2 %all-gather.6.cloned.1.call-start = ((), (), s32[]{:S(2)}) async-start(), calls=%async_computation.5 | async-start | bytes 13369344 | tf_op jit(solution)/shard_map/all_gather | solution.py:305
  9.5 128.0 %all-gather.4.cloned.1.call-start = ((), (), s32[]{:S(2)}) async-start(), calls=%async_computation.4 | async-start | bytes 4456448 | tf_op jit(solution)/shard_map/all_gather | solution.py:307
  26.0 18.0 %all-to-all-start = ((f32[16,64,128]{2,1,0:T(8,128)}), f32[16,64,128]{2,1,0:T(8,128)S(1)}, u32[]{:S(2)}, u32[]{:S(2)}) async-start(f32[16,64,128]{2,1,0:T(8,128)} %broadcast_in_dim.3), calls=%async_computation | async-start | bytes 1048576 | tf_op jit(solution)/shard_map/all_to_all | solution.py:321
  44.0 4.4 %copy-start.2 = (f32[16,64,128]{2,1,0:T(8,128)}, f32[16,64,128]{2,1,0:T(8,128)S(1)}, u32[]{:S(2)}) copy-start(f32[16,64,128]{2,1,0:T(8,128)S(1)} %all-to-all-done.totals_ref) | copy-start | bytes 1572868
  44.0 25.0 %all-to-all-start.2 = ((bf16[16,24,2048]{2,1,0:T(8,128)(2,1)}), bf16[16,24,2048]{2,1,0:T(8,128)(2,1)}, u32[]{:S(2)}, u32[]{:S(2)}) async-start(bf16[16,24,2048]{2,1,0:T(8,128)(2,1)} %bitcast.30), calls=%async_computation.2 | async-start | bytes 3145728 | tf_op jit(solution)/shard_map/all_to_all | solution.py:314
  69.0 34.7 %all-to-all-start.1 = ((bf16[16,64,128]{2,1,0:T(8,128)(2,1)}), bf16[16,64,128]{2,1,0:T(8,128)(2,1)S(1)}, u32[]{:S(2)}, u32[]{:S(2)}) async-start(bf16[16,64,128]{2,1,0:T(8,128)(2,1)} %gate_kernel.1), calls=%async_computation.1 | async-start | bytes 524288 | tf_op jit(solution)/shard_map/all_to_all | solution.py:335
  103.7 7.6 %copy-start.1 = (bf16[128,2048]{1,0:T(8,128)(2,1)S(1)}, bf16[128,2048]{1,0:T(8,128)(2,1)}, u32[]{:S(2)}) copy-start(bf16[128,2048]{1,0:T(8,128)(2,1)} %get-tuple-element.11) | copy-start | bytes 1572868
  103.7 9.7 %copy-start.3 = (bf16[16,64,128]{2,1,0:T(8,128)(2,1)}, bf16[16,64,128]{2,1,0:T(8,128)(2,1)S(1)}, u32[]{:S(2)}) copy-start(bf16[16,64,128]{2,1,0:T(8,128)(2,1)S(1)} %all-to-all-done.1) | copy-start | bytes 786436
  103.7 40.6 %all-to-all-start.3 = ((bf16[16,24,2048]{2,1,0:T(8,128)(2,1)}), bf16[16,24,2048]{2,1,0:T(8,128)(2,1)}, u32[]{:S(2)}, u32[]{:S(2)}) async-start(bf16[16,24,2048]{2,1,0:T(8,128)(2,1)} %expert_kernel.1), calls=%async_computation.3 | async-start | bytes 3145728 | tf_op jit(solution)/shard_map/all_to_all | solution.py:355
Sparse Core Ops, SparseCore 0:
  9.8 84.5 all-gather.5
  96.2 41.2 all-gather.3
where the time goes:
time: 156 us; the launch traced here: 155 us
  waiting for transfers between devices  59.5 us (38%)
  Pallas kernels  39.9 us (26%)
  starting transfers between devices  32.1 us (21%)
  between operations  14.1 us (9%)
  matrix products  5.53 us (4%)
  other arithmetic  2.23 us (1%)
  local copies, waits for them, and re-layouts  1.64 us (1%)
    all_gather x1, waiting for transfers between devices, shards(): projection = lax.all_gather(out_weight, 'tp', axis=0, tiled=True)  20.6 us
    all_to_all x1, waiting for transfers between devices, shards(): lax.all_to_all(sent.reshape(groups, slots, width), EP, split_axis=0, conc...  17.9 us
    pallas_call x1, Pallas kernels, shards(): call(scan_kernel, (shape((2 * dim, length), F32), shape((dim, 2 * dim), F...  14.2 us
    all_gather x1, waiting for transfers between devices, shards(): all_weights = lax.all_gather(local_weights, 'tp')  12.9 us
    all_to_all x1, starting transfers between devices, shards(): lax.all_to_all(rows, 'tp', split_axis=0, concat_axis=0, tiled=True)  12.4 us
    pallas_call x1, Pallas kernels, shards(): call(expert_kernel, shape((groups, slots, width), BF), grid=(2, 2), in_sp...  9.31 us
    all_to_all x1, starting transfers between devices, shards(): lax.all_to_all(results, EP, split_axis=0, concat_axis=0, tiled=True)  7.61 us
    all_to_all x1, starting transfers between devices, shards(): lax.all_to_all(jnp.broadcast_to(total, (groups, dim, 2 * dim)), EP, split...  7.56 us
  transfers between devices with their start and end apart: 6, of which 4 were waited for; matrix products, arithmetic and copies ran while one was open for 5% of the time, Pallas kernels for 23%

commit v1 on v0

--- a/solution.py
+++ b/solution.py
@@ -6,12 +6,13 @@
 from jax.sharding import Mesh
 from jax.sharding import PartitionSpec as P
 
-HEAD_DIM = 64
+
 CHUNK = 128
 GROUP = 4
 SLOTS = 12
 EP = ("ep_0", "ep_1")
-EP_TP = ("ep_0", "ep_1", "tp")
+TP = ("z", "core")
+EP_TP = EP + TP
 BF = jnp.bfloat16
 F32 = jnp.float32
 VMEM_LIMIT = 56 * 1024 * 1024
@@ -102,7 +103,7 @@
             block = jnp.where(near, s["couple"], 0.0)
             s["inv"] = eye + block
             s["power"] = mm(block, block)
-        for step in range(2):
+        for _ in range(2):
             for s in stage:
                 both = mm(jnp.concatenate([s["inv"], s["power"]], axis=0), s["power"])
                 s["inv"] = s["inv"] + both[:n]
@@ -204,69 +205,91 @@
     sent_ref[...] = mm(filled.astype(F32), normed).astype(BF)
 
 
-def expert_kernel(rows_ref, weights_ref, out_ref, sum_ref):
-    e, half = pl.program_id(0), pl.program_id(1)
-    groups, slots, width = rows_ref.shape
+def regroup_kernel(rows_ref, out_ref):
+    rows, width = out_ref.shape[1:]
+    for k in range(3):
+        out_ref[k] = rows_ref[:, 8 * k : 8 * k + 8].reshape(rows, width)
+
+
+def expert_kernel(rows_ref, weights_ref, out_ref, gates_ref, down_ref, hidden_ref, sems, more):
+    groups, _, width = out_ref.shape
     rows = groups * 8
-    hidden = weights_ref.shape[0] * weights_ref.shape[3]
-
-    @pl.when((e == 0) & (half == 0))
-    def _():
-        sum_ref[...] = jnp.zeros_like(sum_ref)
-
-    def go(which):
-        own = rows_ref[:, 8 * which : 8 * which + 8].reshape(rows, width)
-        shared = rows_ref[:, 16:24].reshape(rows, width)
-        given = jnp.concatenate([own, shared], axis=0)
-        gate = dot_dims(given, weights_ref[:, 0, 0].reshape(hidden, width), ((1,), (1,)))
-        upper = dot_dims(given, weights_ref[:, 1, 0].reshape(hidden, width), ((1,), (1,)))
-        act = gate * jax.nn.sigmoid(gate) * upper
-        r = iota(act.shape, 0)
-        mine = (r < rows) | (((r & 7) >= 4) == (which == 1))
-        act = jnp.where(mine, act, 0.0).astype(BF)
-        down = weights_ref[:, 2, 0].reshape(hidden, width)
-        sum_ref[which * rows : (which + 1) * rows] += dot_dims(act[:rows], down, ((1,), (0,)))
-        sum_ref[2 * rows :] += dot_dims(act[rows:], down, ((1,), (0,)))
-
-    @pl.when(e == 0)
-    def _():
-        go(0)
-
-    @pl.when(e == 1)
-    def _():
-        go(1)
-
-    @pl.when((e == 1) & (half == 1))
-    def _():
-        for k in range(3):
-            part = sum_ref[k * rows : (k + 1) * rows].reshape(groups, 8, width)
-            out_ref[:, 8 * k : 8 * k + 8] = part.astype(BF)
-
-
-def combine_kernel(routes_ref, weights_ref, results_ref, shared_ref, out_ref):
-    total = results_ref.shape[0]
+    parts, _, each, units = gates_ref.shape[1:5]
+    n = each * units
+
+    def gates_copy(e, q, w):
+        source = weights_ref.at[pl.ds(q * each, each), w, e]
+        return pltpu.make_async_copy(source, gates_ref.at[e, q, w], sems.at[e, q, w])
+
+    def down_copy(e):
+        return pltpu.make_async_copy(weights_ref.at[:, 2, e], down_ref.at[e], more.at[e])
+
+    for e in range(2):
+        for q in range(parts):
+            for w in range(2):
+                gates_copy(e, q, w).start()
+    for e in range(2):
+        down_copy(e).start()
+    r = iota((2 * rows, n), 0)
+    for e in range(2):
+        given = jnp.concatenate([rows_ref[e], rows_ref[2]], axis=0)
+        mine = (r < rows) | (((r & 7) >= 4) == (e == 1))
+        for q in range(parts):
+            for w in range(2):
+                gates_copy(e, q, w).wait()
+            gates = dot_dims(given, gates_ref[e, q].reshape(2 * n, width), ((1,), (1,)))
+            gate, upper = gates[:, :n], gates[:, n:]
+            act = gate * jax.nn.sigmoid(gate) * upper
+            hidden_ref[e, :, q * n : (q + 1) * n] = jnp.where(mine, act, 0.0).astype(BF)
+    for e in range(2):
+        down_copy(e).wait()
+    step = 512
+    for k in range(0, width, step):
+        at = slice(k, k + step)
+        first, second = (
+            dot_dims(hidden_ref[e], down_ref[e, :, :, at].reshape(parts * n, step), ((1,), (0,)))
+            for e in range(2)
+        )
+        parts_out = (first[:rows], second[:rows], first[rows:] + second[rows:])
+        for j, part in enumerate(parts_out):
+            out_ref[:, 8 * j : 8 * j + 8, at] = part.astype(BF).reshape(groups, 8, step)
+
+
+def table_kernel(routes_ref, weights_ref, out_ref):
+    total = out_ref.shape[2]
     first, second, spread, filled = slot_tables(routes_ref[...], total, total // SLOTS)
     weights = weights_ref[...]
     share = 2.5 * weights / jnp.sum(weights, axis=0, keepdims=True)
     chosen = jnp.where(first, share[0:1], 0.0) + jnp.where(second, share[1:2], 0.0)
     high = chosen.astype(BF).astype(F32)
+    for k, part in enumerate((high, chosen - high)):
+        out_ref[k] = jnp.where(filled, mm(spread, part), 0.0).T.astype(BF)
+
+
+def combine_kernel(tables_ref, results_ref, shared_ref, out_ref):
     results = results_ref[...]
-    out = shared_ref[...]
-    for part in (high, chosen - high):
-        taken = jnp.where(filled, mm(spread, part), 0.0)
-        out = out + mm(taken.T, results)
+    out = shared_ref[...] + (mm(tables_ref[0], results) + mm(tables_ref[1], results))
     out_ref[...] = out.astype(BF)
 
 
-def project_kernel(rows_ref, weight_ref, out_ref):
-    out_ref[...] = dot_dims(rows_ref[...], weight_ref[...], ((0,), (0,))).astype(BF)
+def project_kernel(place_ref, rows_ref, *refs):
+    *blocks, out_ref = refs
+    y, x, core = place_ref[0], place_ref[1], place_ref[2]
+    chips = rows_ref.shape[0]
+    rows = [rows_ref[z, c] for c in range(2) for z in range(chips)]
+    rows = jnp.concatenate(rows, axis=0).T
+    forth = jnp.where(core == 0, 3, 1)
+    for down, way, ref in zip((0, 1, 3, 2), (1, 1, 3, 1), blocks):
+        for right in range(4):
+            at = ((y + forth * down) % 4) * 4 + (x + forth * way * (0, 1, 3, 2)[right]) % 4
+            out = dot_dims(rows, ref[right], ((1,), (0,)))
+            out_ref[:, pl.ds(pl.multiple_of(at * 128, 128), 128)] = out.astype(BF)
 
 
 def call(kernel, out_shape, **options):
     return pl.pallas_call(
         kernel,
         out_shape=out_shape,
-        name=kernel.__name__,
         compiler_params=pltpu.CompilerParams(vmem_limit_bytes=VMEM_LIMIT),
         **options,
     )
@@ -274,6 +297,32 @@
 
 def shape(dims, dtype):
     return jax.ShapeDtypeStruct(dims, dtype)
+
+
+def swap(array, axes):
+    return lax.all_to_all(array, axes, split_axis=0, concat_axis=0, tiled=True)
+
+
+def other_core(array):
+    return lax.ppermute(array, "core", [(0, 1), (1, 0)])
+
+
+def around(block, axis):
+    pairs = [(2 * k, (2 * k + 2) % 8) for k in range(4)]
+    pairs += [((2 * k + 3) % 8, 2 * k + 1) for k in range(4)]
+    came = lax.ppermute(block, (axis, "core"), pairs)
+    more = other_core(came)
+    last = lax.ppermute(came, (axis, "core"), pairs)
+    return [block, came, more, last]
+
+
+def projection_blocks(out_weight, here):
+    columns = out_weight.shape[1] // lax.axis_size(EP)
+    chips = lax.axis_size("z")
+    piece = lax.dynamic_slice_in_dim(out_weight, here * columns, columns, axis=1)
+    heads = swap(jnp.broadcast_to(piece, (chips, *piece.shape)), "z")
+    heads = heads.reshape(-1, columns)
+    return heads
 
 
 def shards(
@@ -296,35 +345,36 @@
     shared_up,
     shared_down,
 ):
-    groups, peers = lax.axis_size(EP), lax.axis_size("tp")
+    groups, peers = lax.axis_size(EP), lax.axis_size(TP)
     here = lax.axis_index(EP)
     length, dim = key_in.shape
     tokens, width = moe_in.shape
 
     local_weights = jnp.stack([w.transpose(0, 2, 1) for w in (expert_gate, expert_up, expert_down)])
-    all_weights = lax.all_gather(local_weights, "tp")
-    out_weight, unused = lax.optimization_barrier((out_weight, local_weights))
-    projection = lax.all_gather(out_weight, "tp", axis=0, tiled=True)
-
+    all_weights = lax.all_gather(local_weights, TP)
+
+    core = lax.axis_index("core")
+    heads = projection_blocks(out_weight, here)
     slots = expert_gate.shape[0] * SLOTS
     normed, sent = call(
         dispatch_kernel,
         (shape((tokens, width), BF), shape((groups * slots, width), BF)),
     )(moe_in, moe_gain.reshape(1, width), routes.T)
-    arrived = lax.all_to_all(
-        sent.reshape(groups, slots, width), EP, split_axis=0, concat_axis=0, tiled=True
+    sent, heads = lax.optimization_barrier((sent, heads))
+    arrived = swap(sent.reshape(groups, slots, width), EP)
+    others = other_core(heads)
+    block = jnp.concatenate(
+        [jnp.where(core == 0, heads, others), jnp.where(core == 0, others, heads)]
     )
-
+    across = jnp.stack(around(block, "ep_1"))
+    projection = around(across, "ep_0")
+
+    key_in, sent = lax.optimization_barrier((key_in, sent))
     reads, total = call(
         scan_kernel, (shape((2 * dim, length), F32), shape((dim, 2 * dim), F32))
     )(key_in.T, receptance.T, payload_vectors.T, decay_in.T, rate_in.T)
-    totals = lax.all_to_all(
-        jnp.broadcast_to(total, (groups, dim, 2 * dim)),
-        EP,
-        split_axis=0,
-        concat_axis=0,
-        tiled=True,
-    )
+    total, arrived = lax.optimization_barrier((total, arrived))
+    totals = swap(jnp.broadcast_to(total, (groups, dim, 2 * dim)), EP)
     smem = pl.BlockSpec(memory_space=pltpu.SMEM)
     vmem = pl.BlockSpec(memory_space=pltpu.VMEM)
     rows = call(
@@ -332,60 +382,60 @@
         shape((peers, dim, length // peers), BF),
         in_specs=[smem] + [vmem] * 4,
     )(here.astype(jnp.int32).reshape(1), totals, reads, gate_in.T, norm_gain.reshape(1, dim))
-    token_rows = lax.all_to_all(rows, "tp", split_axis=0, concat_axis=0, tiled=True)
+    token_rows = swap(rows, TP)
 
     gate = jnp.dot(normed, shared_gate, preferred_element_type=F32)
     upper = jnp.dot(normed, shared_up, preferred_element_type=F32)
     hidden = (jax.nn.silu(gate) * upper).astype(BF)
     shared_term = jnp.dot(hidden, shared_down, preferred_element_type=F32)
 
-    part = peers // 2
     units = expert_gate.shape[2]
+    each = 4
+    given = call(regroup_kernel, shape((3, groups * 8, width), BF))(arrived)
+    tables = call(table_kernel, shape((2, tokens, groups * slots), BF))(routes.T, route_weights.T)
     results = call(
         expert_kernel,
         shape((groups, slots, width), BF),
-        grid=(2, 2),
-        in_specs=[
-            pl.BlockSpec((groups, slots, width), lambda e, h: (0, 0, 0)),
-            pl.BlockSpec((part, 3, 1, units, width), lambda e, h: (h, 0, e, 0, 0)),
+        in_specs=[vmem, pl.BlockSpec(memory_space=pl.ANY)],
+        scratch_shapes=[
+            pltpu.VMEM((2, peers // each, 2, each, units, width), BF),
+            pltpu.VMEM((2, peers, units, width), BF),
+            pltpu.VMEM((2, groups * 16, peers * units), BF),
+            pltpu.SemaphoreType.DMA((2, peers // each, 2)),
+            pltpu.SemaphoreType.DMA((2,)),
         ],
-        out_specs=pl.BlockSpec((groups, slots, width), lambda e, h: (0, 0, 0)),
-        scratch_shapes=[pltpu.VMEM((groups * slots, width), F32)],
-    )(arrived, all_weights)
-    returned = lax.all_to_all(results, EP, split_axis=0, concat_axis=0, tiled=True)
+    )(given, all_weights)
+    results, token_rows = lax.optimization_barrier((results, token_rows))
+    returned = swap(results, EP)
     moe_out = call(combine_kernel, shape((tokens, width), BF))(
-        routes.T, route_weights.T, returned.reshape(groups * slots, width), shared_term
+        tables, returned.reshape(groups * slots, width), shared_term
     )
 
-    columns = width // 8
+    place = jnp.stack([lax.axis_index(axis) for axis in EP] + [core]).astype(jnp.int32)
     mixed = call(
         project_kernel,
         shape((tokens, width), BF),
-        grid=(width // columns,),
-        in_specs=[
-            pl.BlockSpec((peers * dim, tokens), lambda i: (0, 0)),
-            pl.BlockSpec((peers * dim, columns), lambda i: (0, i)),
-        ],
-        out_specs=pl.BlockSpec((tokens, columns), lambda i: (0, i)),
-    )(token_rows.reshape(peers * dim, tokens), projection)
+        in_specs=[smem] + [vmem] * (1 + len(projection)),
+    )(place, token_rows.reshape(peers // 2, 2, dim, tokens), *projection)
     return (mixed, moe_out)
 
 
 def solution(mesh):
-    torus = Mesh(mesh.devices.reshape(4, 4, mesh.shape["tp"]), ("ep_0", "ep_1", "tp"))
+    torus = Mesh(mesh.devices.reshape(4, 4, mesh.shape["tp"] // 2, 2), EP_TP)
     placed = (
-        *(P(EP, "tp"),) * 6,
-        P("tp"),
-        P("tp", None),
+        *(P(EP, TP),) * 6,
+        P(TP),
+        P(TP, None),
         P(EP_TP, None),
         P(),
         P(EP_TP, None),
         P(EP_TP, None),
-        *(P(EP, None, "tp"),) * 3,
+        *(P(EP, None, TP),) * 3,
         P(),
         P(),
         P(),
     )
+
     return jax.shard_map(
         shards,
         mesh=torus,

time: 156 us -> 164 us (1.051)
  starting transfers between devices: 32.1 us -> 45.1 us
  waiting for transfers between devices: 59.5 us -> 47.2 us
  Pallas kernels: 39.9 us -> 43.3 us
  local copies, waits for them, and re-layouts: 1.64 us -> 3.78 us
  other arithmetic: 2.23 us -> 4.16 us
    ppermute x0 -> x7, waiting for transfers between devices: none -> 36.1 us  [the longest x2 19.3 us: around(): last = lax.ppermute(came, (axis, 'core'), pairs)]
    all_gather x2 -> x1, waiting for transfers between devices: 33.6 us -> 0.01 us  [shards(): all_weights = lax.all_gather(local_weights, TP)]
    all_to_all x4 -> x5, waiting for transfers between devices: 25.2 us -> 11.1 us  [swap(): return lax.all_to_all(array, axes, split_axis=0, concat_axis=0, tiled=True)]
    ppermute x0 -> x7, starting transfers between devices: none -> 13.3 us  [the longest x2 5.33 us: around(): came = lax.ppermute(block, (axis, 'core'), pairs)]
    pallas_call x2 -> x4, Pallas kernels: 16.1 us -> 20 us  [the longest x1 11.1 us: shards(): call(expert_kernel, shape((groups, slots, width), BF), in_specs=[vmem, pl...]
    another operation x0 -> x3, other arithmetic: none -> 1.88 us  [the longest x2 1.28 us: shards(): across = jnp.stack(around(block, 'ep_1'))]
    all_to_all x4 -> x5, starting transfers between devices: 32 us -> 31.7 us  [swap(): return lax.all_to_all(array, axes, split_axis=0, concat_axis=0, tiled=True)]
  transfers between devices with their start and end apart: 6 -> 13, of which waited for: 4 -> 5; matrix products, arithmetic and copies ran while one was open for 5% -> 6% of each run, Pallas kernels for 23% -> 24%
where the time goes in v1:
time: 164 us; the launch traced here: 163 us
  waiting for transfers between devices  47.2 us (29%)
  starting transfers between devices  45.1 us (28%)
  Pallas kernels  43.3 us (26%)
  between operations  14.2 us (9%)
  matrix products  5.6 us (3%)
  other arithmetic  4.16 us (3%)
  local copies, waits for them, and re-layouts  3.78 us (2%)
    all_to_all x5, starting transfers between devices, swap(): return lax.all_to_all(array, axes, split_axis=0, concat_axis=0, tiled=True)  31.7 us
    ppermute x2, waiting for transfers between devices, around(): last = lax.ppermute(came, (axis, 'core'), pairs)  19.3 us
    ppermute x2, waiting for transfers between devices, around(): came = lax.ppermute(block, (axis, 'core'), pairs)  15.7 us
    pallas_call x1, Pallas kernels, shards(): call(scan_kernel, (shape((2 * dim, length), F32), shape((dim, 2 * dim), F...  14.2 us
    pallas_call x1, Pallas kernels, shards(): call(expert_kernel, shape((groups, slots, width), BF), in_specs=[vmem, pl...  11.1 us
    all_to_all x5, waiting for transfers between devices, swap(): return lax.all_to_all(array, axes, split_axis=0, concat_axis=0, tiled=True)  11.1 us
    ppermute x2, starting transfers between devices, around(): came = lax.ppermute(block, (axis, 'core'), pairs)  5.33 us
    ppermute x3, starting transfers between devices, other_core(): return lax.ppermute(array, 'core', [(0, 1), (1, 0)])  4.75 us
  transfers between devices with their start and end apart: 13, of which 5 were waited for; matrix products, arithmetic and copies ran while one was open for 6% of the time, Pallas kernels for 24%

profile of v1, /device:TPU:1, one launch (start us, length us, event | category | flops | bytes accessed | tf_op | source)
XLA Modules:
  0.0 163.3 jit_solution(1950609588010031639)
XLA Ops:
  7.2 2.3 %pad_maximum_fusion.1 = bf16[3,2,32,2048]{3,2,1,0:T(8,128)(2,1)} fusion(bf16[1,2,32,2048]{3,2,1,0:T(8,128)(2,1)} %bitcast.48, bf16[1,2,32,2048]{3,2,1,0:T(8,128)(2,1)} %bitcast.49, bf16[1,2,32,2048]{3,2,1,0:T(8,128)(2,1)} %bitcast.50), kind=kLoop, calls=%fused_computation.4 | loop fusion | flops 786432 | bytes 1572864 | tf_op jit(solution)/shard_map/stack | solution.py:353
  9.5 0.7 constant_dynamic-slice_fusion
  10.2 0.7 broadcast_in_dim.6
  10.9 9.0 %all-to-all-start = ((bf16[8,64,128]{2,1,0:T(8,128)(2,1)}), bf16[8,64,128]{2,1,0:T(8,128)(2,1)S(1)}, u32[]{:S(2)}, u32[]{:S(2)}) async-start(bf16[8,64,128]{2,1,0:T(8,128)(2,1)} %broadcast_in_dim.6), calls=%async_computation | async-start | bytes 262144 | tf_op jit(solution)/shard_map/all_to_all | solution.py:303
  19.9 3.2 %shard_map.185 = (bf16[128,2048]{1,0:T(8,128)(2,1)}, bf16[384,2048]{1,0:T(8,128)(2,1)}) custom-call(bf16[128,2048]{1,0:T(8,128)(2,1)} %moe_ref.1, f32[1,2048]{1,0:T(1,128)} %bitcast.55, s32[2,128]{1,0:T(2,128)} %bitcast.56), custom_call_target="tpu_custom_call" | custom-call | tf_op jit(solution)/shard_map/pallas_call | solution.py:359
  23.1 4.6 %all-to-all-done = bf16[8,64,128]{2,1,0:T(8,128)(2,1)S(1)} async-done(((bf16[8,64,128]{2,1,0:T(8,128)(2,1)}), bf16[8,64,128]{2,1,0:T(8,128)(2,1)S(1)}, u32[]{:S(2)}, u32[]{:S(2)}) %all-to-all-start) | async-done | bytes 131104 | tf_op jit(solution)/shard_map/all_to_all | solution.py:303
  27.7 6.8 %all-to-all-start.1 = ((bf16[16,24,2048]{2,1,0:T(8,128)(2,1)}), bf16[16,24,2048]{2,1,0:T(8,128)(2,1)}, u32[]{:S(2)}, u32[]{:S(2)}) async-start(bf16[16,24,2048]{2,1,0:T(8,128)(2,1)} %bitcast.39), calls=%async_computation.1 | async-start | bytes 3145728 | tf_op jit(solution)/shard_map/all_to_all | solution.py:303
  34.5 2.8 %collective-permute-start = (bf16[512,128]{1,0:T(8,128)(2,1)S(1)}, bf16[512,128]{1,0:T(8,128)(2,1)S(1)}, u32[]{:S(2)}, u32[]{:S(2)}) collective-permute-start(bf16[512,128]{1,0:T(8,128)(2,1)S(1)} %bitcast.41), channel_id=1, source_target_pairs={{0,1},{1,0},{2,3},{3,2},{4,5},{5,4},{6,7},{7,6},{8,9},{9,8},{10,11... | collective-permute-start | bytes 393224 | tf_op jit(solution)/shard_map/ppermute | solution.py:307
  37.2 1.1 collective-permute-done
  38.4 2.7 %collective-permute-start.1 = (bf16[1024,128]{1,0:T(8,128)(2,1)S(1)}, bf16[1024,128]{1,0:T(8,128)(2,1)S(1)}, u32[]{:S(2)}, u32[]{:S(2)}) collective-permute-start(bf16[1024,128]{1,0:T(8,128)(2,1)S(1)} %get-tuple-element.25), channel_id=1, source_target_pairs={{0,16},{16,32},{32,48},{48,0},{17,1},{33,17},{49,33},{1,49},{2,18}... | collective-permute-start | bytes 786440 | tf_op jit(solution)/shard_map/ppermute | solution.py:313
  41.1 15.7 %collective-permute-done.1 = bf16[1024,128]{1,0:T(8,128)(2,1)S(1)} collective-permute-done((bf16[1024,128]{1,0:T(8,128)(2,1)S(1)}, bf16[1024,128]{1,0:T(8,128)(2,1)S(1)}, u32[]{:S(2)}, u32[]{:S(2)}) %collective-permute-start.1) | collective-permute-done | bytes 262176 | tf_op jit(solution)/shard_map/ppermute | solution.py:313
  57.3 1.2 collective-permute-start.2
  58.5 14.2 %shard_map.186 = (f32[128,2048]{1,0:T(8,128)}, f32[64,128]{1,0:T(8,128)}) custom-call(bf16[64,2048]{1,0:T(8,128)(2,1)} %bitcast.43, bf16[64,2048]{1,0:T(8,128)(2,1)} %bitcast.44, bf16[64,2048]{1,0:T(8,128)(2,1)} %bitcast.45, bf16[64,2048]{1,0:T(8,128)(2,1)} %bitcast.46, bf16[64,2048]{1,0:T(8,128)(2,1)} %bitcast.47), custom_call_target="tpu_custom_call" | custom-call | tf_op jit(solution)/shard_map/pallas_call | solution.py:373
  72.7 1.6 broadcast_in_dim.7
  74.3 6.8 %all-to-all-start.2 = ((f32[16,64,128]{2,1,0:T(8,128)}), f32[16,64,128]{2,1,0:T(8,128)}, u32[]{:S(2)}, u32[]{:S(2)}) async-start(f32[16,64,128]{2,1,0:T(8,128)} %broadcast_in_dim.7), calls=%async_computation.2 | async-start | bytes 1048576 | tf_op jit(solution)/shard_map/all_to_all | solution.py:303
  81.2 0.7 copy-done.5
  81.9 1.2 pad_maximum_fusion.refs_0_
  83.2 2.6 %collective-permute-start.4 = (bf16[4,1024,128]{2,1,0:T(8,128)(2,1)S(1)}, bf16[4,1024,128]{2,1,0:T(8,128)(2,1)}, u32[]{:S(2)}, u32[]{:S(2)}) collective-permute-start(bf16[4,1024,128]{2,1,0:T(8,128)(2,1)S(1)} %pad_maximum_fusion.refs_0_), channel_id=1, source_target_pairs={{0,64},{64,128},{128,192},{192,0},{65,1},{129,65},{193,129},{1,193... | collective-permute-start | bytes 3145736 | tf_op jit(solution)/shard_map/ppermute | solution.py:313
  85.8 6.5 %all-to-all-done.2.totals_ref = f32[16,64,128]{2,1,0:T(8,128)} async-done(((f32[16,64,128]{2,1,0:T(8,128)}), f32[16,64,128]{2,1,0:T(8,128)}, u32[]{:S(2)}, u32[]{:S(2)}) %all-to-all-start.2) | async-done | bytes 524320 | tf_op jit(solution)/shard_map/all_to_all | solution.py:303
  92.3 2.6 %shard_map.189 = bf16[16,64,128]{2,1,0:T(8,128)(2,1)} custom-call(s32[1]{0:T(128)} %bitcast.19.here_ref, f32[16,64,128]{2,1,0:T(8,128)} %all-to-all-done.2.totals_ref, f32[128,2048]{1,0:T(8,128)} %get-tuple-element.19.reads_ref, bf16[64,2048]{1,0:T(8,128)(2,1)} %bitcast.51, f32[1,64]{1,0:T(1,128)} %bitcast.59), custom_call_target="tpu_custom_call" | custom-call | tf_op jit(solution)/shard_map/pallas_call | solution.py:380
  94.9 4.7 %all-to-all-start.3 = ((bf16[16,64,128]{2,1,0:T(8,128)(2,1)}), bf16[16,64,128]{2,1,0:T(8,128)(2,1)S(1)}, u32[]{:S(2)}, u32[]{:S(2)}) async-start(bf16[16,64,128]{2,1,0:T(8,128)(2,1)} %shard_map.189), calls=%async_computation.3 | async-start | bytes 524288 | tf_op jit(solution)/shard_map/all_to_all | solution.py:303
  99.6 2.7 %shard_map.187.rows_ref = bf16[3,128,2048]{2,1,0:T(8,128)(2,1)} custom-call(bf16[16,24,2048]{2,1,0:T(8,128)(2,1)} %all-to-all-done.1.rows_ref), custom_call_target="tpu_custom_call" | custom-call | tf_op jit(solution)/shard_map/pallas_call | solution.py:394
  102.3 11.1 %shard_map.188 = bf16[16,24,2048]{2,1,0:T(8,128)(2,1)} custom-call(bf16[3,128,2048]{2,1,0:T(8,128)(2,1)} %shard_map.187.rows_ref, bf16[16,3,2,32,2048]{4,3,2,1,0:T(8,128)(2,1)} %bitcast.38), custom_call_target="tpu_custom_call" | custom-call | tf_op jit(solution)/shard_map/pallas_call | solution.py:396
  113.4 4.4 %all-to-all-start.4 = ((bf16[16,24,2048]{2,1,0:T(8,128)(2,1)}), bf16[16,24,2048]{2,1,0:T(8,128)(2,1)}, u32[]{:S(2)}, u32[]{:S(2)}) async-start(bf16[16,24,2048]{2,1,0:T(8,128)(2,1)} %shard_map.188), calls=%async_computation.4 | async-start | bytes 3145728 | tf_op jit(solution)/shard_map/all_to_all | solution.py:303
  117.9 0.8 collective-permute-start.5
  118.7 2.8 %collective-permute-start.6 = (bf16[4,1024,128]{2,1,0:T(8,128)(2,1)}, bf16[4,1024,128]{2,1,0:T(8,128)(2,1)}, u32[]{:S(2)}, u32[]{:S(2)}) collective-permute-start(bf16[4,1024,128]{2,1,0:T(8,128)(2,1)} %collective-permute-done.4.refs_1_), channel_id=1, source_target_pairs={{0,64},{64,128},{128,192},{192,0},{65,1},{129,65},{193,129},{1,193... | collective-permute-start | bytes 3145736 | tf_op jit(solution)/shard_map/ppermute | solution.py:315
  121.5 1.8 %shard_map.191.tables_ref = bf16[2,128,384]{2,1,0:T(8,128)(2,1)} custom-call(s32[2,128]{1,0:T(2,128)} %bitcast.57, f32[2,128]{1,0:T(2,128)} %bitcast.58), custom_call_target="tpu_custom_call" | custom-call | tf_op jit(solution)/shard_map/pallas_call | solution.py:395
  123.9 2.2 %fusion.10 = f32[128,512]{1,0:T(8,128)S(1)} fusion(bf16[128,2048]{1,0:T(8,128)(2,1)} %get-tuple-element.23, bf16[2048,512]{1,0:T(8,128)(2,1)} %param.33), kind=kOutput, calls=%fused_computation.18 | convolution fusion | flops 268435456 | bytes 2883584 | tf_op jit(solution)/shard_map/dot_general | solution.py:387
  126.2 3.4 %fusion.1.shared_ref = f32[128,2048]{1,0:T(8,128)} fusion(bf16[512,2048]{1,0:T(8,128)(2,1)S(1)} %copy-done, bf16[128,2048]{1,0:T(8,128)(2,1)S(1)} %copy-done.2, bf16[2048,512]{1,0:T(8,128)(2,1)} %param.34, f32[128,512]{1,0:T(8,128)S(1)} %fusion.10), kind=kOutput, calls=%fused_computation.2 | convolution fusion | flops 537264128 | bytes 6029312 | tf_op jit(solution)/shard_map/dot_general | solution.py:390
  129.6 19.3 %collective-permute-done.6.refs_3_ = bf16[4,1024,128]{2,1,0:T(8,128)(2,1)} collective-permute-done((bf16[4,1024,128]{2,1,0:T(8,128)(2,1)}, bf16[4,1024,128]{2,1,0:T(8,128)(2,1)}, u32[]{:S(2)}, u32[]{:S(2)}) %collective-permute-start.6) | collective-permute-done | bytes 1048608 | tf_op jit(solution)/shard_map/ppermute | solution.py:315
  148.9 4.4 %shard_map.190 = bf16[128,2048]{1,0:T(8,128)(2,1)} custom-call(s32[3]{0:T(128)} %pad_add_fusion.place_ref, bf16[8,2,64,128]{3,2,1,0:T(8,128)(2,1)} %bitcast.40, bf16[4,1024,128]{2,1,0:T(8,128)(2,1)} %copy-done.1, bf16[4,1024,128]{2,1,0:T(8,128)(2,1)} %collective-permute-done.4.refs_1_, bf16[4,1024,128]{2,1,0:T(8,128)(2,1)} %collective-permute-done.5.refs_2_, ...), custom_call_target="tpu_custom_call" | custom-call | tf_op jit(solution)/shard_map/pallas_call | solution.py:415
  153.2 3.3 %shard_map.192 = bf16[128,2048]{1,0:T(8,128)(2,1)} custom-call(bf16[2,128,384]{2,1,0:T(8,128)(2,1)} %shard_map.191.tables_ref, bf16[384,2048]{1,0:T(8,128)(2,1)} %bitcast.28.results_ref, f32[128,2048]{1,0:T(8,128)} %fusion.1.shared_ref), custom_call_target="tpu_custom_call" | custom-call | tf_op jit(solution)/shard_map/pallas_call | solution.py:410
  (27 shorter events, 1.3 us)
Async XLA Ops:
  7.2 119.0 %copy-start = (bf16[512,2048]{1,0:T(8,128)(2,1)S(1)}, bf16[512,2048]{1,0:T(8,128)(2,1)}, u32[]{:S(2)}) copy-start(bf16[512,2048]{1,0:T(8,128)(2,1)} %param.35) | copy-start | bytes 6291460
  7.2 95.1 %all-gather.3.cloned.1.call-start = ((), (), s32[]{:S(2)}) async-start(), calls=%async_computation.5 | async-start | bytes 13369344 | tf_op jit(solution)/shard_map/all_gather | solution.py:354
  10.9 16.8 %all-to-all-start = ((bf16[8,64,128]{2,1,0:T(8,128)(2,1)}), bf16[8,64,128]{2,1,0:T(8,128)(2,1)S(1)}, u32[]{:S(2)}, u32[]{:S(2)}) async-start(bf16[8,64,128]{2,1,0:T(8,128)(2,1)} %broadcast_in_dim.6), calls=%async_computation | async-start | bytes 262144 | tf_op jit(solution)/shard_map/all_to_all | solution.py:303
  27.7 45.1 %all-to-all-start.1 = ((bf16[16,24,2048]{2,1,0:T(8,128)(2,1)}), bf16[16,24,2048]{2,1,0:T(8,128)(2,1)}, u32[]{:S(2)}, u32[]{:S(2)}) async-start(bf16[16,24,2048]{2,1,0:T(8,128)(2,1)} %bitcast.39), calls=%async_computation.1 | async-start | bytes 3145728 | tf_op jit(solution)/shard_map/all_to_all | solution.py:303
  34.5 3.9 %collective-permute-start = (bf16[512,128]{1,0:T(8,128)(2,1)S(1)}, bf16[512,128]{1,0:T(8,128)(2,1)S(1)}, u32[]{:S(2)}, u32[]{:S(2)}) collective-permute-start(bf16[512,128]{1,0:T(8,128)(2,1)S(1)} %bitcast.41), channel_id=1, source_target_pairs={{0,1},{1,0},{2,3},{3,2},{4,5},{5,4},{6,7},{7,6},{8,9},{9,8},{10,11... | collective-permute-start | bytes 393224 | tf_op jit(solution)/shard_map/ppermute | solution.py:307
  38.4 18.5 %collective-permute-start.1 = (bf16[1024,128]{1,0:T(8,128)(2,1)S(1)}, bf16[1024,128]{1,0:T(8,128)(2,1)S(1)}, u32[]{:S(2)}, u32[]{:S(2)}) collective-permute-start(bf16[1024,128]{1,0:T(8,128)(2,1)S(1)} %get-tuple-element.25), channel_id=1, source_target_pairs={{0,16},{16,32},{32,48},{48,0},{17,1},{33,17},{49,33},{1,49},{2,18}... | collective-permute-start | bytes 786440 | tf_op jit(solution)/shard_map/ppermute | solution.py:313
  56.9 24.3 %copy-start.4 = (bf16[1024,128]{1,0:T(8,128)(2,1)}, bf16[1024,128]{1,0:T(8,128)(2,1)S(1)}, u32[]{:S(2)}) copy-start(bf16[1024,128]{1,0:T(8,128)(2,1)S(1)} %collective-permute-done.1) | copy-start | bytes 786436
  56.9 24.3 %collective-permute-start.3 = (bf16[1024,128]{1,0:T(8,128)(2,1)S(1)}, bf16[1024,128]{1,0:T(8,128)(2,1)S(1)}, u32[]{:S(2)}, u32[]{:S(2)}) collective-permute-start(bf16[1024,128]{1,0:T(8,128)(2,1)S(1)} %collective-permute-done.1), channel_id=1, source_target_pairs={{0,16},{16,32},{32,48},{48,0},{17,1},{33,17},{49,33},{1,49},{2,18}... | collective-permute-start | bytes 786440 | tf_op jit(solution)/shard_map/ppermute | solution.py:315
  57.3 23.8 %collective-permute-start.2 = (bf16[1024,128]{1,0:T(8,128)(2,1)S(1)}, bf16[1024,128]{1,0:T(8,128)(2,1)S(1)}, u32[]{:S(2)}, u32[]{:S(2)}) collective-permute-start(bf16[1024,128]{1,0:T(8,128)(2,1)S(1)} %collective-permute-done.1), channel_id=1, source_target_pairs={{0,1},{1,0},{2,3},{3,2},{4,5},{5,4},{6,7},{7,6},{8,9},{9,8},{10,11... | collective-permute-start | bytes 786440 | tf_op jit(solution)/shard_map/ppermute | solution.py:307
  74.3 17.9 %all-to-all-start.2 = ((f32[16,64,128]{2,1,0:T(8,128)}), f32[16,64,128]{2,1,0:T(8,128)}, u32[]{:S(2)}, u32[]{:S(2)}) async-start(f32[16,64,128]{2,1,0:T(8,128)} %broadcast_in_dim.7), calls=%async_computation.2 | async-start | bytes 1048576 | tf_op jit(solution)/shard_map/all_to_all | solution.py:303
  81.1 0.7 copy-start.5
  81.2 0.8 copy-start.6
  83.2 19.1 %copy-start.1 = (bf16[4,1024,128]{2,1,0:T(8,128)(2,1)}, bf16[4,1024,128]{2,1,0:T(8,128)(2,1)S(1)}, u32[]{:S(2)}) copy-start(bf16[4,1024,128]{2,1,0:T(8,128)(2,1)S(1)} %pad_maximum_fusion.refs_0_) | copy-start | bytes 3145732
  83.2 34.7 %collective-permute-start.4 = (bf16[4,1024,128]{2,1,0:T(8,128)(2,1)S(1)}, bf16[4,1024,128]{2,1,0:T(8,128)(2,1)}, u32[]{:S(2)}, u32[]{:S(2)}) collective-permute-start(bf16[4,1024,128]{2,1,0:T(8,128)(2,1)S(1)} %pad_maximum_fusion.refs_0_), channel_id=1, source_target_pairs={{0,64},{64,128},{128,192},{192,0},{65,1},{129,65},{193,129},{1,193... | collective-permute-start | bytes 3145736 | tf_op jit(solution)/shard_map/ppermute | solution.py:313
  94.9 18.5 %all-to-all-start.3 = ((bf16[16,64,128]{2,1,0:T(8,128)(2,1)}), bf16[16,64,128]{2,1,0:T(8,128)(2,1)S(1)}, u32[]{:S(2)}, u32[]{:S(2)}) async-start(bf16[16,64,128]{2,1,0:T(8,128)(2,1)} %shard_map.189), calls=%async_computation.3 | async-start | bytes 524288 | tf_op jit(solution)/shard_map/all_to_all | solution.py:303
  113.4 12.7 %copy-start.3 = (bf16[16,64,128]{2,1,0:T(8,128)(2,1)}, bf16[16,64,128]{2,1,0:T(8,128)(2,1)S(1)}, u32[]{:S(2)}) copy-start(bf16[16,64,128]{2,1,0:T(8,128)(2,1)S(1)} %all-to-all-done.3) | copy-start | bytes 786436
  113.4 39.8 %all-to-all-start.4 = ((bf16[16,24,2048]{2,1,0:T(8,128)(2,1)}), bf16[16,24,2048]{2,1,0:T(8,128)(2,1)}, u32[]{:S(2)}, u32[]{:S(2)}) async-start(bf16[16,24,2048]{2,1,0:T(8,128)(2,1)} %shard_map.188), calls=%async_computation.4 | async-start | bytes 3145728 | tf_op jit(solution)/shard_map/all_to_all | solution.py:303
  117.9 8.3 %copy-start.2 = (bf16[128,2048]{1,0:T(8,128)(2,1)S(1)}, bf16[128,2048]{1,0:T(8,128)(2,1)}, u32[]{:S(2)}) copy-start(bf16[128,2048]{1,0:T(8,128)(2,1)} %get-tuple-element.23) | copy-start | bytes 1572868
  117.9 11.7 %collective-permute-start.5 = (bf16[4,1024,128]{2,1,0:T(8,128)(2,1)}, bf16[4,1024,128]{2,1,0:T(8,128)(2,1)}, u32[]{:S(2)}, u32[]{:S(2)}) collective-permute-start(bf16[4,1024,128]{2,1,0:T(8,128)(2,1)} %collective-permute-done.4.refs_1_), channel_id=1, source_target_pairs={{0,1},{1,0},{2,3},{3,2},{4,5},{5,4},{6,7},{7,6},{8,9},{9,8},{10,11... | collective-permute-start | bytes 3145736 | tf_op jit(solution)/shard_map/ppermute | solution.py:307
  118.7 30.2 %collective-permute-start.6 = (bf16[4,1024,128]{2,1,0:T(8,128)(2,1)}, bf16[4,1024,128]{2,1,0:T(8,128)(2,1)}, u32[]{:S(2)}, u32[]{:S(2)}) collective-permute-start(bf16[4,1024,128]{2,1,0:T(8,128)(2,1)} %collective-permute-done.4.refs_1_), channel_id=1, source_target_pairs={{0,64},{64,128},{128,192},{192,0},{65,1},{129,65},{193,129},{1,193... | collective-permute-start | bytes 3145736 | tf_op jit(solution)/shard_map/ppermute | solution.py:315
Sparse Core Ops, SparseCore 0:
  9.8 79.9 all-gather.2

commit v2 on v1

--- a/solution.py
+++ b/solution.py
@@ -206,53 +206,45 @@
 
 
 def regroup_kernel(rows_ref, out_ref):
-    rows, width = out_ref.shape[1:]
-    for k in range(3):
-        out_ref[k] = rows_ref[:, 8 * k : 8 * k + 8].reshape(rows, width)
-
-
-def expert_kernel(rows_ref, weights_ref, out_ref, gates_ref, down_ref, hidden_ref, sems, more):
+    rows, width = out_ref.shape[1] // 2, out_ref.shape[2]
+    both = rows_ref[:, 16:24].reshape(rows, width)
+    for e in range(2):
+        out_ref[e, :rows] = rows_ref[:, 8 * e : 8 * e + 8].reshape(rows, width)
+        out_ref[e, rows:] = both
+
+
+def expert_kernel(given_ref, gates_ref, down_ref, out_ref, hidden_ref, sum_ref):
+    e, h = pl.program_id(0), pl.program_id(1)
     groups, _, width = out_ref.shape
     rows = groups * 8
-    parts, _, each, units = gates_ref.shape[1:5]
-    n = each * units
-
-    def gates_copy(e, q, w):
-        source = weights_ref.at[pl.ds(q * each, each), w, e]
-        return pltpu.make_async_copy(source, gates_ref.at[e, q, w], sems.at[e, q, w])
-
-    def down_copy(e):
-        return pltpu.make_async_copy(weights_ref.at[:, 2, e], down_ref.at[e], more.at[e])
-
-    for e in range(2):
-        for q in range(parts):
-            for w in range(2):
-                gates_copy(e, q, w).start()
-    for e in range(2):
-        down_copy(e).start()
-    r = iota((2 * rows, n), 0)
-    for e in range(2):
-        given = jnp.concatenate([rows_ref[e], rows_ref[2]], axis=0)
-        mine = (r < rows) | (((r & 7) >= 4) == (e == 1))
-        for q in range(parts):
-            for w in range(2):
-                gates_copy(e, q, w).wait()
-            gates = dot_dims(given, gates_ref[e, q].reshape(2 * n, width), ((1,), (1,)))
-            gate, upper = gates[:, :n], gates[:, n:]
-            act = gate * jax.nn.sigmoid(gate) * upper
-            hidden_ref[e, :, q * n : (q + 1) * n] = jnp.where(mine, act, 0.0).astype(BF)
-    for e in range(2):
-        down_copy(e).wait()
+    n = gates_ref.shape[0] * gates_ref.shape[3]
+    given = given_ref[0]
+    gate = dot_dims(given, gates_ref[:, 0, 0].reshape(n, width), ((1,), (1,)))
+    upper = dot_dims(given, gates_ref[:, 1, 0].reshape(n, width), ((1,), (1,)))
+    act = gate * jax.nn.sigmoid(gate) * upper
+    r = iota(act.shape, 0)
+    act = jnp.where((r < rows) | (((r & 7) >> 2) == e), act, 0.0)
+    hidden_ref[:, pl.ds(pl.multiple_of(h * n, n), n)] = act.astype(BF)
     step = 512
-    for k in range(0, width, step):
-        at = slice(k, k + step)
-        first, second = (
-            dot_dims(hidden_ref[e], down_ref[e, :, :, at].reshape(parts * n, step), ((1,), (0,)))
-            for e in range(2)
-        )
-        parts_out = (first[:rows], second[:rows], first[rows:] + second[rows:])
-        for j, part in enumerate(parts_out):
-            out_ref[:, 8 * j : 8 * j + 8, at] = part.astype(BF).reshape(groups, 8, step)
+
+    def finish(which):
+        for k in range(0, width, step):
+            at = slice(k, k + step)
+            down = down_ref[:, 0, 0, :, at].reshape(hidden_ref.shape[1], step)
+            out = dot_dims(hidden_ref[...], down, ((1,), (0,)))
+            own = out[:rows].astype(BF).reshape(groups, 8, step)
+            out_ref[:, 8 * which : 8 * which + 8, at] = own
+            if which == 0:
+                sum_ref[:, at] = out[rows:]
+            else:
+                both = (sum_ref[:, at] + out[rows:]).astype(BF)
+                out_ref[:, 16:24, at] = both.reshape(groups, 8, step)
+
+    for which in range(2):
+
+        @pl.when((e == which) & (h == 1))
+        def _():
+            finish(which)
 
 
 def table_kernel(routes_ref, weights_ref, out_ref):
@@ -390,21 +382,23 @@
     shared_term = jnp.dot(hidden, shared_down, preferred_element_type=F32)
 
     units = expert_gate.shape[2]
-    each = 4
-    given = call(regroup_kernel, shape((3, groups * 8, width), BF))(arrived)
+    given = call(regroup_kernel, shape((2, groups * 16, width), BF))(arrived)
     tables = call(table_kernel, shape((2, tokens, groups * slots), BF))(routes.T, route_weights.T)
     results = call(
         expert_kernel,
         shape((groups, slots, width), BF),
-        in_specs=[vmem, pl.BlockSpec(memory_space=pl.ANY)],
+        grid=(2, 2),
+        in_specs=[
+            pl.BlockSpec((1, groups * 16, width), lambda e, h: (e, 0, 0)),
+            pl.BlockSpec((peers // 2, 2, 1, units, width), lambda e, h: (h, 0, e, 0, 0)),
+            pl.BlockSpec((peers, 1, 1, units, width), lambda e, h: (0, 2, e, 0, 0)),
+        ],
+        out_specs=pl.BlockSpec((groups, slots, width), lambda e, h: (0, 0, 0)),
         scratch_shapes=[
-            pltpu.VMEM((2, peers // each, 2, each, units, width), BF),
-            pltpu.VMEM((2, peers, units, width), BF),
-            pltpu.VMEM((2, groups * 16, peers * units), BF),
-            pltpu.SemaphoreType.DMA((2, peers // each, 2)),
-            pltpu.SemaphoreType.DMA((2,)),
+            pltpu.VMEM((groups * 16, peers * units), BF),
+            pltpu.VMEM((groups * 8, width), F32),
         ],
-    )(given, all_weights)
+    )(given, all_weights, all_weights)
     results, token_rows = lax.optimization_barrier((results, token_rows))
     returned = swap(results, EP)
     moe_out = call(combine_kernel, shape((tokens, width), BF))(

time: 164 us -> 163 us (level)
  no operation moved by 1% of the time
where the time goes in v2:
time: 163 us; the launch traced here: 162 us
  waiting for transfers between devices  47.4 us (29%)
  starting transfers between devices  44.9 us (28%)
  Pallas kernels  41.7 us (26%)
  between operations  14.2 us (9%)
  matrix products  5.6 us (3%)
  other arithmetic  4.16 us (3%)
  local copies, waits for them, and re-layouts  3.78 us (2%)
    all_to_all x5, starting transfers between devices, swap(): return lax.all_to_all(array, axes, split_axis=0, concat_axis=0, tiled=True)  31.7 us
    ppermute x2, waiting for transfers between devices, around(): last = lax.ppermute(came, (axis, 'core'), pairs)  19.5 us
    ppermute x2, waiting for transfers between devices, around(): came = lax.ppermute(block, (axis, 'core'), pairs)  15.7 us
    pallas_call x1, Pallas kernels, shards(): call(scan_kernel, (shape((2 * dim, length), F32), shape((dim, 2 * dim), F...  14.2 us
    all_to_all x5, waiting for transfers between devices, swap(): return lax.all_to_all(array, axes, split_axis=0, concat_axis=0, tiled=True)  11.1 us
    pallas_call x1, Pallas kernels, shards(): call(expert_kernel, shape((groups, slots, width), BF), grid=(2, 2), in_sp...  9.35 us
    ppermute x2, starting transfers between devices, around(): came = lax.ppermute(block, (axis, 'core'), pairs)  5.33 us
    ppermute x3, starting transfers between devices, other_core(): return lax.ppermute(array, 'core', [(0, 1), (1, 0)])  4.56 us
  transfers between devices with their start and end apart: 13, of which 5 were waited for; matrix products, arithmetic and copies ran while one was open for 6% of the time, Pallas kernels for 24%

profile of v2, /device:TPU:1, one launch (start us, length us, event | category | flops | bytes accessed | tf_op | source)
XLA Modules:
  0.0 161.7 jit_solution(18193819351021528822)
XLA Ops:
  7.2 2.3 %pad_maximum_fusion.1 = bf16[3,2,32,2048]{3,2,1,0:T(8,128)(2,1)} fusion(bf16[1,2,32,2048]{3,2,1,0:T(8,128)(2,1)} %bitcast.49, bf16[1,2,32,2048]{3,2,1,0:T(8,128)(2,1)} %bitcast.50, bf16[1,2,32,2048]{3,2,1,0:T(8,128)(2,1)} %bitcast.51), kind=kLoop, calls=%fused_computation.4 | loop fusion | flops 786432 | bytes 1572864 | tf_op jit(solution)/shard_map/stack | solution.py:345
  9.5 0.7 constant_dynamic-slice_fusion
  10.2 0.7 broadcast_in_dim.6
  10.9 9.0 %all-to-all-start = ((bf16[8,64,128]{2,1,0:T(8,128)(2,1)}), bf16[8,64,128]{2,1,0:T(8,128)(2,1)S(1)}, u32[]{:S(2)}, u32[]{:S(2)}) async-start(bf16[8,64,128]{2,1,0:T(8,128)(2,1)} %broadcast_in_dim.6), calls=%async_computation | async-start | bytes 262144 | tf_op jit(solution)/shard_map/all_to_all | solution.py:295
  19.9 3.2 %shard_map.185 = (bf16[128,2048]{1,0:T(8,128)(2,1)}, bf16[384,2048]{1,0:T(8,128)(2,1)}) custom-call(bf16[128,2048]{1,0:T(8,128)(2,1)} %moe_ref.1, f32[1,2048]{1,0:T(1,128)} %bitcast.56, s32[2,128]{1,0:T(2,128)} %bitcast.57), custom_call_target="tpu_custom_call" | custom-call | tf_op jit(solution)/shard_map/pallas_call | solution.py:351
  23.1 4.6 %all-to-all-done = bf16[8,64,128]{2,1,0:T(8,128)(2,1)S(1)} async-done(((bf16[8,64,128]{2,1,0:T(8,128)(2,1)}), bf16[8,64,128]{2,1,0:T(8,128)(2,1)S(1)}, u32[]{:S(2)}, u32[]{:S(2)}) %all-to-all-start) | async-done | bytes 131104 | tf_op jit(solution)/shard_map/all_to_all | solution.py:295
  27.7 6.8 %all-to-all-start.1 = ((bf16[16,24,2048]{2,1,0:T(8,128)(2,1)}), bf16[16,24,2048]{2,1,0:T(8,128)(2,1)}, u32[]{:S(2)}, u32[]{:S(2)}) async-start(bf16[16,24,2048]{2,1,0:T(8,128)(2,1)} %bitcast.40), calls=%async_computation.1 | async-start | bytes 3145728 | tf_op jit(solution)/shard_map/all_to_all | solution.py:295
  34.5 2.8 %collective-permute-start = (bf16[512,128]{1,0:T(8,128)(2,1)S(1)}, bf16[512,128]{1,0:T(8,128)(2,1)S(1)}, u32[]{:S(2)}, u32[]{:S(2)}) collective-permute-start(bf16[512,128]{1,0:T(8,128)(2,1)S(1)} %bitcast.42), channel_id=1, source_target_pairs={{0,1},{1,0},{2,3},{3,2},{4,5},{5,4},{6,7},{7,6},{8,9},{9,8},{10,11... | collective-permute-start | bytes 393224 | tf_op jit(solution)/shard_map/ppermute | solution.py:299
  37.2 1.1 collective-permute-done
  38.4 2.7 %collective-permute-start.1 = (bf16[1024,128]{1,0:T(8,128)(2,1)S(1)}, bf16[1024,128]{1,0:T(8,128)(2,1)S(1)}, u32[]{:S(2)}, u32[]{:S(2)}) collective-permute-start(bf16[1024,128]{1,0:T(8,128)(2,1)S(1)} %get-tuple-element.25), channel_id=1, source_target_pairs={{0,16},{16,32},{32,48},{48,0},{17,1},{33,17},{49,33},{1,49},{2,18}... | collective-permute-start | bytes 786440 | tf_op jit(solution)/shard_map/ppermute | solution.py:305
  41.1 15.7 %collective-permute-done.1 = bf16[1024,128]{1,0:T(8,128)(2,1)S(1)} collective-permute-done((bf16[1024,128]{1,0:T(8,128)(2,1)S(1)}, bf16[1024,128]{1,0:T(8,128)(2,1)S(1)}, u32[]{:S(2)}, u32[]{:S(2)}) %collective-permute-start.1) | collective-permute-done | bytes 262176 | tf_op jit(solution)/shard_map/ppermute | solution.py:305
  57.3 1.2 collective-permute-start.2
  58.5 14.2 %shard_map.186 = (f32[128,2048]{1,0:T(8,128)}, f32[64,128]{1,0:T(8,128)}) custom-call(bf16[64,2048]{1,0:T(8,128)(2,1)} %bitcast.44, bf16[64,2048]{1,0:T(8,128)(2,1)} %bitcast.45, bf16[64,2048]{1,0:T(8,128)(2,1)} %bitcast.46, bf16[64,2048]{1,0:T(8,128)(2,1)} %bitcast.47, bf16[64,2048]{1,0:T(8,128)(2,1)} %bitcast.48), custom_call_target="tpu_custom_call" | custom-call | tf_op jit(solution)/shard_map/pallas_call | solution.py:365
  72.7 1.6 broadcast_in_dim.7
  74.3 6.8 %all-to-all-start.2 = ((f32[16,64,128]{2,1,0:T(8,128)}), f32[16,64,128]{2,1,0:T(8,128)}, u32[]{:S(2)}, u32[]{:S(2)}) async-start(f32[16,64,128]{2,1,0:T(8,128)} %broadcast_in_dim.7), calls=%async_computation.2 | async-start | bytes 1048576 | tf_op jit(solution)/shard_map/all_to_all | solution.py:295
  81.2 0.7 copy-done.5
  81.9 1.2 pad_maximum_fusion.refs_0_
  83.2 2.6 %collective-permute-start.4 = (bf16[4,1024,128]{2,1,0:T(8,128)(2,1)S(1)}, bf16[4,1024,128]{2,1,0:T(8,128)(2,1)}, u32[]{:S(2)}, u32[]{:S(2)}) collective-permute-start(bf16[4,1024,128]{2,1,0:T(8,128)(2,1)S(1)} %pad_maximum_fusion.refs_0_), channel_id=1, source_target_pairs={{0,64},{64,128},{128,192},{192,0},{65,1},{129,65},{193,129},{1,193... | collective-permute-start | bytes 3145736 | tf_op jit(solution)/shard_map/ppermute | solution.py:305
  85.8 6.5 %all-to-all-done.2.totals_ref = f32[16,64,128]{2,1,0:T(8,128)} async-done(((f32[16,64,128]{2,1,0:T(8,128)}), f32[16,64,128]{2,1,0:T(8,128)}, u32[]{:S(2)}, u32[]{:S(2)}) %all-to-all-start.2) | async-done | bytes 524320 | tf_op jit(solution)/shard_map/all_to_all | solution.py:295
  92.3 2.6 %shard_map.189 = bf16[16,64,128]{2,1,0:T(8,128)(2,1)} custom-call(s32[1]{0:T(128)} %bitcast.19.here_ref, f32[16,64,128]{2,1,0:T(8,128)} %all-to-all-done.2.totals_ref, f32[128,2048]{1,0:T(8,128)} %get-tuple-element.19.reads_ref, bf16[64,2048]{1,0:T(8,128)(2,1)} %bitcast.52, f32[1,64]{1,0:T(1,128)} %bitcast.60), custom_call_target="tpu_custom_call" | custom-call | tf_op jit(solution)/shard_map/pallas_call | solution.py:372
  94.9 4.7 %all-to-all-start.3 = ((bf16[16,64,128]{2,1,0:T(8,128)(2,1)}), bf16[16,64,128]{2,1,0:T(8,128)(2,1)S(1)}, u32[]{:S(2)}, u32[]{:S(2)}) async-start(bf16[16,64,128]{2,1,0:T(8,128)(2,1)} %shard_map.189), calls=%async_computation.3 | async-start | bytes 524288 | tf_op jit(solution)/shard_map/all_to_all | solution.py:295
  99.6 2.9 %shard_map.187.given_ref = bf16[2,256,2048]{2,1,0:T(8,128)(2,1)} custom-call(bf16[16,24,2048]{2,1,0:T(8,128)(2,1)} %all-to-all-done.1.rows_ref), custom_call_target="tpu_custom_call" | custom-call | tf_op jit(solution)/shard_map/pallas_call | solution.py:385
  102.5 9.3 %shard_map.188 = bf16[16,24,2048]{2,1,0:T(8,128)(2,1)} custom-call(bf16[2,256,2048]{2,1,0:T(8,128)(2,1)} %shard_map.187.given_ref, bf16[16,3,2,32,2048]{4,3,2,1,0:T(8,128)(2,1)} %bitcast.38, bf16[16,3,2,32,2048]{4,3,2,1,0:T(8,128)(2,1)} %bitcast.39), custom_call_target="tpu_custom_call" | custom-call | tf_op jit(solution)/shard_map/pallas_call | solution.py:387
  111.8 4.4 %all-to-all-start.4 = ((bf16[16,24,2048]{2,1,0:T(8,128)(2,1)}), bf16[16,24,2048]{2,1,0:T(8,128)(2,1)}, u32[]{:S(2)}, u32[]{:S(2)}) async-start(bf16[16,24,2048]{2,1,0:T(8,128)(2,1)} %shard_map.188), calls=%async_computation.4 | async-start | bytes 3145728 | tf_op jit(solution)/shard_map/all_to_all | solution.py:295
  116.9 2.8 %collective-permute-start.6 = (bf16[4,1024,128]{2,1,0:T(8,128)(2,1)}, bf16[4,1024,128]{2,1,0:T(8,128)(2,1)}, u32[]{:S(2)}, u32[]{:S(2)}) collective-permute-start(bf16[4,1024,128]{2,1,0:T(8,128)(2,1)} %collective-permute-done.4.refs_1_), channel_id=1, source_target_pairs={{0,64},{64,128},{128,192},{192,0},{65,1},{129,65},{193,129},{1,193... | collective-permute-start | bytes 3145736 | tf_op jit(solution)/shard_map/ppermute | solution.py:307
  119.7 1.8 %shard_map.191.tables_ref = bf16[2,128,384]{2,1,0:T(8,128)(2,1)} custom-call(s32[2,128]{1,0:T(2,128)} %bitcast.58, f32[2,128]{1,0:T(2,128)} %bitcast.59), custom_call_target="tpu_custom_call" | custom-call | tf_op jit(solution)/shard_map/pallas_call | solution.py:386
  121.5 0.6 pad_add_fusion.place_ref
  122.1 2.2 %fusion.10 = f32[128,512]{1,0:T(8,128)S(1)} fusion(bf16[128,2048]{1,0:T(8,128)(2,1)} %get-tuple-element.23, bf16[2048,512]{1,0:T(8,128)(2,1)} %param.33), kind=kOutput, calls=%fused_computation.18 | convolution fusion | flops 268435456 | bytes 2883584 | tf_op jit(solution)/shard_map/dot_general | solution.py:379
  124.4 3.4 %fusion.1.shared_ref = f32[128,2048]{1,0:T(8,128)} fusion(bf16[512,2048]{1,0:T(8,128)(2,1)S(1)} %copy-done, bf16[128,2048]{1,0:T(8,128)(2,1)S(1)} %copy-done.2, bf16[2048,512]{1,0:T(8,128)(2,1)} %param.34, f32[128,512]{1,0:T(8,128)S(1)} %fusion.10), kind=kOutput, calls=%fused_computation.2 | convolution fusion | flops 537264128 | bytes 6029312 | tf_op jit(solution)/shard_map/dot_general | solution.py:382
  127.8 19.5 %collective-permute-done.6.refs_3_ = bf16[4,1024,128]{2,1,0:T(8,128)(2,1)} collective-permute-done((bf16[4,1024,128]{2,1,0:T(8,128)(2,1)}, bf16[4,1024,128]{2,1,0:T(8,128)(2,1)}, u32[]{:S(2)}, u32[]{:S(2)}) %collective-permute-start.6) | collective-permute-done | bytes 1048608 | tf_op jit(solution)/shard_map/ppermute | solution.py:307
  147.3 4.4 %shard_map.190 = bf16[128,2048]{1,0:T(8,128)(2,1)} custom-call(s32[3]{0:T(128)} %pad_add_fusion.place_ref, bf16[8,2,64,128]{3,2,1,0:T(8,128)(2,1)} %bitcast.41, bf16[4,1024,128]{2,1,0:T(8,128)(2,1)} %copy-done.1, bf16[4,1024,128]{2,1,0:T(8,128)(2,1)} %collective-permute-done.4.refs_1_, bf16[4,1024,128]{2,1,0:T(8,128)(2,1)} %collective-permute-done.5.refs_2_, ...), custom_call_target="tpu_custom_call" | custom-call | tf_op jit(solution)/shard_map/pallas_call | solution.py:409
  151.6 3.3 %shard_map.192 = bf16[128,2048]{1,0:T(8,128)(2,1)} custom-call(bf16[2,128,384]{2,1,0:T(8,128)(2,1)} %shard_map.191.tables_ref, bf16[384,2048]{1,0:T(8,128)(2,1)} %bitcast.28.results_ref, f32[128,2048]{1,0:T(8,128)} %fusion.1.shared_ref), custom_call_target="tpu_custom_call" | custom-call | tf_op jit(solution)/shard_map/pallas_call | solution.py:404
  (27 shorter events, 1.3 us)
Async XLA Ops:
  7.2 117.2 %copy-start = (bf16[512,2048]{1,0:T(8,128)(2,1)S(1)}, bf16[512,2048]{1,0:T(8,128)(2,1)}, u32[]{:S(2)}) copy-start(bf16[512,2048]{1,0:T(8,128)(2,1)} %param.35) | copy-start | bytes 6291460
  7.2 95.3 %all-gather.3.cloned.1.call-start = ((), (), s32[]{:S(2)}) async-start(), calls=%async_computation.5 | async-start | bytes 13369344 | tf_op jit(solution)/shard_map/all_gather | solution.py:346
  10.9 16.8 %all-to-all-start = ((bf16[8,64,128]{2,1,0:T(8,128)(2,1)}), bf16[8,64,128]{2,1,0:T(8,128)(2,1)S(1)}, u32[]{:S(2)}, u32[]{:S(2)}) async-start(bf16[8,64,128]{2,1,0:T(8,128)(2,1)} %broadcast_in_dim.6), calls=%async_computation | async-start | bytes 262144 | tf_op jit(solution)/shard_map/all_to_all | solution.py:295
  27.7 45.1 %all-to-all-start.1 = ((bf16[16,24,2048]{2,1,0:T(8,128)(2,1)}), bf16[16,24,2048]{2,1,0:T(8,128)(2,1)}, u32[]{:S(2)}, u32[]{:S(2)}) async-start(bf16[16,24,2048]{2,1,0:T(8,128)(2,1)} %bitcast.40), calls=%async_computation.1 | async-start | bytes 3145728 | tf_op jit(solution)/shard_map/all_to_all | solution.py:295
  34.5 3.9 %collective-permute-start = (bf16[512,128]{1,0:T(8,128)(2,1)S(1)}, bf16[512,128]{1,0:T(8,128)(2,1)S(1)}, u32[]{:S(2)}, u32[]{:S(2)}) collective-permute-start(bf16[512,128]{1,0:T(8,128)(2,1)S(1)} %bitcast.42), channel_id=1, source_target_pairs={{0,1},{1,0},{2,3},{3,2},{4,5},{5,4},{6,7},{7,6},{8,9},{9,8},{10,11... | collective-permute-start | bytes 393224 | tf_op jit(solution)/shard_map/ppermute | solution.py:299
  38.4 18.5 %collective-permute-start.1 = (bf16[1024,128]{1,0:T(8,128)(2,1)S(1)}, bf16[1024,128]{1,0:T(8,128)(2,1)S(1)}, u32[]{:S(2)}, u32[]{:S(2)}) collective-permute-start(bf16[1024,128]{1,0:T(8,128)(2,1)S(1)} %get-tuple-element.25), channel_id=1, source_target_pairs={{0,16},{16,32},{32,48},{48,0},{17,1},{33,17},{49,33},{1,49},{2,18}... | collective-permute-start | bytes 786440 | tf_op jit(solution)/shard_map/ppermute | solution.py:305
  56.9 24.3 %copy-start.4 = (bf16[1024,128]{1,0:T(8,128)(2,1)}, bf16[1024,128]{1,0:T(8,128)(2,1)S(1)}, u32[]{:S(2)}) copy-start(bf16[1024,128]{1,0:T(8,128)(2,1)S(1)} %collective-permute-done.1) | copy-start | bytes 786436
  56.9 24.3 %collective-permute-start.3 = (bf16[1024,128]{1,0:T(8,128)(2,1)S(1)}, bf16[1024,128]{1,0:T(8,128)(2,1)S(1)}, u32[]{:S(2)}, u32[]{:S(2)}) collective-permute-start(bf16[1024,128]{1,0:T(8,128)(2,1)S(1)} %collective-permute-done.1), channel_id=1, source_target_pairs={{0,16},{16,32},{32,48},{48,0},{17,1},{33,17},{49,33},{1,49},{2,18}... | collective-permute-start | bytes 786440 | tf_op jit(solution)/shard_map/ppermute | solution.py:307
  57.3 23.8 %collective-permute-start.2 = (bf16[1024,128]{1,0:T(8,128)(2,1)S(1)}, bf16[1024,128]{1,0:T(8,128)(2,1)S(1)}, u32[]{:S(2)}, u32[]{:S(2)}) collective-permute-start(bf16[1024,128]{1,0:T(8,128)(2,1)S(1)} %collective-permute-done.1), channel_id=1, source_target_pairs={{0,1},{1,0},{2,3},{3,2},{4,5},{5,4},{6,7},{7,6},{8,9},{9,8},{10,11... | collective-permute-start | bytes 786440 | tf_op jit(solution)/shard_map/ppermute | solution.py:299
  74.3 17.9 %all-to-all-start.2 = ((f32[16,64,128]{2,1,0:T(8,128)}), f32[16,64,128]{2,1,0:T(8,128)}, u32[]{:S(2)}, u32[]{:S(2)}) async-start(f32[16,64,128]{2,1,0:T(8,128)} %broadcast_in_dim.7), calls=%async_computation.2 | async-start | bytes 1048576 | tf_op jit(solution)/shard_map/all_to_all | solution.py:295
  81.1 0.7 copy-start.5
  81.2 0.8 copy-start.6
  83.2 19.3 %copy-start.1 = (bf16[4,1024,128]{2,1,0:T(8,128)(2,1)}, bf16[4,1024,128]{2,1,0:T(8,128)(2,1)S(1)}, u32[]{:S(2)}) copy-start(bf16[4,1024,128]{2,1,0:T(8,128)(2,1)S(1)} %pad_maximum_fusion.refs_0_) | copy-start | bytes 3145732
  83.2 33.1 %collective-permute-start.4 = (bf16[4,1024,128]{2,1,0:T(8,128)(2,1)S(1)}, bf16[4,1024,128]{2,1,0:T(8,128)(2,1)}, u32[]{:S(2)}, u32[]{:S(2)}) collective-permute-start(bf16[4,1024,128]{2,1,0:T(8,128)(2,1)S(1)} %pad_maximum_fusion.refs_0_), channel_id=1, source_target_pairs={{0,64},{64,128},{128,192},{192,0},{65,1},{129,65},{193,129},{1,193... | collective-permute-start | bytes 3145736 | tf_op jit(solution)/shard_map/ppermute | solution.py:305
  94.9 17.0 %all-to-all-start.3 = ((bf16[16,64,128]{2,1,0:T(8,128)(2,1)}), bf16[16,64,128]{2,1,0:T(8,128)(2,1)S(1)}, u32[]{:S(2)}, u32[]{:S(2)}) async-start(bf16[16,64,128]{2,1,0:T(8,128)(2,1)} %shard_map.189), calls=%async_computation.3 | async-start | bytes 524288 | tf_op jit(solution)/shard_map/all_to_all | solution.py:295
  111.8 12.5 %copy-start.3 = (bf16[16,64,128]{2,1,0:T(8,128)(2,1)}, bf16[16,64,128]{2,1,0:T(8,128)(2,1)S(1)}, u32[]{:S(2)}) copy-start(bf16[16,64,128]{2,1,0:T(8,128)(2,1)S(1)} %all-to-all-done.3) | copy-start | bytes 786436
  111.8 39.8 %all-to-all-start.4 = ((bf16[16,24,2048]{2,1,0:T(8,128)(2,1)}), bf16[16,24,2048]{2,1,0:T(8,128)(2,1)}, u32[]{:S(2)}, u32[]{:S(2)}) async-start(bf16[16,24,2048]{2,1,0:T(8,128)(2,1)} %shard_map.188), calls=%async_computation.4 | async-start | bytes 3145728 | tf_op jit(solution)/shard_map/all_to_all | solution.py:295
  116.3 8.1 %copy-start.2 = (bf16[128,2048]{1,0:T(8,128)(2,1)S(1)}, bf16[128,2048]{1,0:T(8,128)(2,1)}, u32[]{:S(2)}) copy-start(bf16[128,2048]{1,0:T(8,128)(2,1)} %get-tuple-element.23) | copy-start | bytes 1572868
  116.3 11.5 %collective-permute-start.5 = (bf16[4,1024,128]{2,1,0:T(8,128)(2,1)}, bf16[4,1024,128]{2,1,0:T(8,128)(2,1)}, u32[]{:S(2)}, u32[]{:S(2)}) collective-permute-start(bf16[4,1024,128]{2,1,0:T(8,128)(2,1)} %collective-permute-done.4.refs_1_), channel_id=1, source_target_pairs={{0,1},{1,0},{2,3},{3,2},{4,5},{5,4},{6,7},{7,6},{8,9},{9,8},{10,11... | collective-permute-start | bytes 3145736 | tf_op jit(solution)/shard_map/ppermute | solution.py:299
  116.9 30.4 %collective-permute-start.6 = (bf16[4,1024,128]{2,1,0:T(8,128)(2,1)}, bf16[4,1024,128]{2,1,0:T(8,128)(2,1)}, u32[]{:S(2)}, u32[]{:S(2)}) collective-permute-start(bf16[4,1024,128]{2,1,0:T(8,128)(2,1)} %collective-permute-done.4.refs_1_), channel_id=1, source_target_pairs={{0,64},{64,128},{128,192},{192,0},{65,1},{129,65},{193,129},{1,193... | collective-permute-start | bytes 3145736 | tf_op jit(solution)/shard_map/ppermute | solution.py:307
Sparse Core Ops, SparseCore 0:
  9.8 79.9 all-gather.2

commit v3 on v2

--- a/solution.py
+++ b/solution.py
@@ -213,11 +213,21 @@
         out_ref[e, rows:] = both
 
 
-def expert_kernel(given_ref, gates_ref, down_ref, out_ref, hidden_ref, sum_ref):
+def expert_kernel(given_ref, gates_ref, weights_ref, out_ref, down_ref, hidden_ref, sum_ref, sems):
     e, h = pl.program_id(0), pl.program_id(1)
     groups, _, width = out_ref.shape
     rows = groups * 8
     n = gates_ref.shape[0] * gates_ref.shape[3]
+
+    def down_copy(which):
+        source = weights_ref.at[:, 2, which]
+        return pltpu.make_async_copy(source, down_ref.at[which], sems.at[which])
+
+    @pl.when((e == 0) & (h == 0))
+    def _():
+        down_copy(0).start()
+        down_copy(1).start()
+
     given = given_ref[0]
     gate = dot_dims(given, gates_ref[:, 0, 0].reshape(n, width), ((1,), (1,)))
     upper = dot_dims(given, gates_ref[:, 1, 0].reshape(n, width), ((1,), (1,)))
@@ -228,9 +238,10 @@
     step = 512
 
     def finish(which):
+        down_copy(which).wait()
         for k in range(0, width, step):
             at = slice(k, k + step)
-            down = down_ref[:, 0, 0, :, at].reshape(hidden_ref.shape[1], step)
+            down = down_ref[which, :, :, at].reshape(hidden_ref.shape[1], step)
             out = dot_dims(hidden_ref[...], down, ((1,), (0,)))
             own = out[:rows].astype(BF).reshape(groups, 8, step)
             out_ref[:, 8 * which : 8 * which + 8, at] = own
@@ -391,12 +402,14 @@
         in_specs=[
             pl.BlockSpec((1, groups * 16, width), lambda e, h: (e, 0, 0)),
             pl.BlockSpec((peers // 2, 2, 1, units, width), lambda e, h: (h, 0, e, 0, 0)),
-            pl.BlockSpec((peers, 1, 1, units, width), lambda e, h: (0, 2, e, 0, 0)),
+            pl.BlockSpec(memory_space=pl.ANY),
         ],
         out_specs=pl.BlockSpec((groups, slots, width), lambda e, h: (0, 0, 0)),
         scratch_shapes=[
+            pltpu.VMEM((2, peers, units, width), BF),
             pltpu.VMEM((groups * 16, peers * units), BF),
             pltpu.VMEM((groups * 8, width), F32),
+            pltpu.SemaphoreType.DMA((2,)),
         ],
     )(given, all_weights, all_weights)
     results, token_rows = lax.optimization_barrier((results, token_rows))

time: 163 us -> 162 us (level)
  transfers between devices with their start and end apart: 13 -> 13, of which waited for: 5 -> 5; matrix products, arithmetic and copies ran while one was open for 6% -> 7% of each run, Pallas kernels for 24% -> 23%
where the time goes in v3:
time: 162 us; the launch traced here: 161 us
  waiting for transfers between devices  47.4 us (29%)
  starting transfers between devices  44.9 us (28%)
  Pallas kernels  41.2 us (25%)
  between operations  14.2 us (9%)
  matrix products  5.6 us (3%)
  other arithmetic  4.16 us (3%)
  local copies, waits for them, and re-layouts  3.78 us (2%)
    all_to_all x5, starting transfers between devices, swap(): return lax.all_to_all(array, axes, split_axis=0, concat_axis=0, tiled=True)  31.7 us
    ppermute x2, waiting for transfers between devices, around(): last = lax.ppermute(came, (axis, 'core'), pairs)  19.5 us
    ppermute x2, waiting for transfers between devices, around(): came = lax.ppermute(block, (axis, 'core'), pairs)  15.7 us
    pallas_call x1, Pallas kernels, shards(): call(scan_kernel, (shape((2 * dim, length), F32), shape((dim, 2 * dim), F...  14.2 us
    all_to_all x5, waiting for transfers between devices, swap(): return lax.all_to_all(array, axes, split_axis=0, concat_axis=0, tiled=True)  11.1 us
    pallas_call x1, Pallas kernels, shards(): call(expert_kernel, shape((groups, slots, width), BF), grid=(2, 2), in_sp...  8.84 us
    ppermute x2, starting transfers between devices, around(): came = lax.ppermute(block, (axis, 'core'), pairs)  5.33 us
    ppermute x3, starting transfers between devices, other_core(): return lax.ppermute(array, 'core', [(0, 1), (1, 0)])  4.56 us
  transfers between devices with their start and end apart: 13, of which 5 were waited for; matrix products, arithmetic and copies ran while one was open for 7% of the time, Pallas kernels for 23%

profile of v3, /device:TPU:1, one launch (start us, length us, event | category | flops | bytes accessed | tf_op | source)
XLA Modules:
  0.0 161.3 jit_solution(14681829287122229040)
XLA Ops:
  7.2 2.3 %pad_maximum_fusion.1 = bf16[3,2,32,2048]{3,2,1,0:T(8,128)(2,1)} fusion(bf16[1,2,32,2048]{3,2,1,0:T(8,128)(2,1)} %bitcast.49, bf16[1,2,32,2048]{3,2,1,0:T(8,128)(2,1)} %bitcast.50, bf16[1,2,32,2048]{3,2,1,0:T(8,128)(2,1)} %bitcast.51), kind=kLoop, calls=%fused_computation.4 | loop fusion | flops 786432 | bytes 1572864 | tf_op jit(solution)/shard_map/stack | solution.py:356
  9.5 0.7 constant_dynamic-slice_fusion
  10.2 0.7 broadcast_in_dim.6
  10.9 9.0 %all-to-all-start = ((bf16[8,64,128]{2,1,0:T(8,128)(2,1)}), bf16[8,64,128]{2,1,0:T(8,128)(2,1)S(1)}, u32[]{:S(2)}, u32[]{:S(2)}) async-start(bf16[8,64,128]{2,1,0:T(8,128)(2,1)} %broadcast_in_dim.6), calls=%async_computation | async-start | bytes 262144 | tf_op jit(solution)/shard_map/all_to_all | solution.py:306
  19.9 3.2 %shard_map.185 = (bf16[128,2048]{1,0:T(8,128)(2,1)}, bf16[384,2048]{1,0:T(8,128)(2,1)}) custom-call(bf16[128,2048]{1,0:T(8,128)(2,1)} %moe_ref.1, f32[1,2048]{1,0:T(1,128)} %bitcast.56, s32[2,128]{1,0:T(2,128)} %bitcast.57), custom_call_target="tpu_custom_call" | custom-call | tf_op jit(solution)/shard_map/pallas_call | solution.py:362
  23.1 4.6 %all-to-all-done = bf16[8,64,128]{2,1,0:T(8,128)(2,1)S(1)} async-done(((bf16[8,64,128]{2,1,0:T(8,128)(2,1)}), bf16[8,64,128]{2,1,0:T(8,128)(2,1)S(1)}, u32[]{:S(2)}, u32[]{:S(2)}) %all-to-all-start) | async-done | bytes 131104 | tf_op jit(solution)/shard_map/all_to_all | solution.py:306
  27.7 6.8 %all-to-all-start.1 = ((bf16[16,24,2048]{2,1,0:T(8,128)(2,1)}), bf16[16,24,2048]{2,1,0:T(8,128)(2,1)}, u32[]{:S(2)}, u32[]{:S(2)}) async-start(bf16[16,24,2048]{2,1,0:T(8,128)(2,1)} %bitcast.40), calls=%async_computation.1 | async-start | bytes 3145728 | tf_op jit(solution)/shard_map/all_to_all | solution.py:306
  34.5 2.8 %collective-permute-start = (bf16[512,128]{1,0:T(8,128)(2,1)S(1)}, bf16[512,128]{1,0:T(8,128)(2,1)S(1)}, u32[]{:S(2)}, u32[]{:S(2)}) collective-permute-start(bf16[512,128]{1,0:T(8,128)(2,1)S(1)} %bitcast.42), channel_id=1, source_target_pairs={{0,1},{1,0},{2,3},{3,2},{4,5},{5,4},{6,7},{7,6},{8,9},{9,8},{10,11... | collective-permute-start | bytes 393224 | tf_op jit(solution)/shard_map/ppermute | solution.py:310
  37.2 1.1 collective-permute-done
  38.4 2.7 %collective-permute-start.1 = (bf16[1024,128]{1,0:T(8,128)(2,1)S(1)}, bf16[1024,128]{1,0:T(8,128)(2,1)S(1)}, u32[]{:S(2)}, u32[]{:S(2)}) collective-permute-start(bf16[1024,128]{1,0:T(8,128)(2,1)S(1)} %get-tuple-element.25), channel_id=1, source_target_pairs={{0,16},{16,32},{32,48},{48,0},{17,1},{33,17},{49,33},{1,49},{2,18}... | collective-permute-start | bytes 786440 | tf_op jit(solution)/shard_map/ppermute | solution.py:316
  41.1 15.7 %collective-permute-done.1 = bf16[1024,128]{1,0:T(8,128)(2,1)S(1)} collective-permute-done((bf16[1024,128]{1,0:T(8,128)(2,1)S(1)}, bf16[1024,128]{1,0:T(8,128)(2,1)S(1)}, u32[]{:S(2)}, u32[]{:S(2)}) %collective-permute-start.1) | collective-permute-done | bytes 262176 | tf_op jit(solution)/shard_map/ppermute | solution.py:316
  57.3 1.2 collective-permute-start.2
  58.5 14.2 %shard_map.186 = (f32[128,2048]{1,0:T(8,128)}, f32[64,128]{1,0:T(8,128)}) custom-call(bf16[64,2048]{1,0:T(8,128)(2,1)} %bitcast.44, bf16[64,2048]{1,0:T(8,128)(2,1)} %bitcast.45, bf16[64,2048]{1,0:T(8,128)(2,1)} %bitcast.46, bf16[64,2048]{1,0:T(8,128)(2,1)} %bitcast.47, bf16[64,2048]{1,0:T(8,128)(2,1)} %bitcast.48), custom_call_target="tpu_custom_call" | custom-call | tf_op jit(solution)/shard_map/pallas_call | solution.py:376
  72.7 1.6 broadcast_in_dim.7
  74.3 6.8 %all-to-all-start.2 = ((f32[16,64,128]{2,1,0:T(8,128)}), f32[16,64,128]{2,1,0:T(8,128)}, u32[]{:S(2)}, u32[]{:S(2)}) async-start(f32[16,64,128]{2,1,0:T(8,128)} %broadcast_in_dim.7), calls=%async_computation.2 | async-start | bytes 1048576 | tf_op jit(solution)/shard_map/all_to_all | solution.py:306
  81.2 0.7 copy-done.5
  81.9 1.2 pad_maximum_fusion.refs_0_
  83.2 2.6 %collective-permute-start.4 = (bf16[4,1024,128]{2,1,0:T(8,128)(2,1)S(1)}, bf16[4,1024,128]{2,1,0:T(8,128)(2,1)}, u32[]{:S(2)}, u32[]{:S(2)}) collective-permute-start(bf16[4,1024,128]{2,1,0:T(8,128)(2,1)S(1)} %pad_maximum_fusion.refs_0_), channel_id=1, source_target_pairs={{0,64},{64,128},{128,192},{192,0},{65,1},{129,65},{193,129},{1,193... | collective-permute-start | bytes 3145736 | tf_op jit(solution)/shard_map/ppermute | solution.py:316
  85.8 6.5 %all-to-all-done.2.totals_ref = f32[16,64,128]{2,1,0:T(8,128)} async-done(((f32[16,64,128]{2,1,0:T(8,128)}), f32[16,64,128]{2,1,0:T(8,128)}, u32[]{:S(2)}, u32[]{:S(2)}) %all-to-all-start.2) | async-done | bytes 524320 | tf_op jit(solution)/shard_map/all_to_all | solution.py:306
  92.3 2.6 %shard_map.189 = bf16[16,64,128]{2,1,0:T(8,128)(2,1)} custom-call(s32[1]{0:T(128)} %bitcast.19.here_ref, f32[16,64,128]{2,1,0:T(8,128)} %all-to-all-done.2.totals_ref, f32[128,2048]{1,0:T(8,128)} %get-tuple-element.19.reads_ref, bf16[64,2048]{1,0:T(8,128)(2,1)} %bitcast.52, f32[1,64]{1,0:T(1,128)} %bitcast.60), custom_call_target="tpu_custom_call" | custom-call | tf_op jit(solution)/shard_map/pallas_call | solution.py:383
  94.9 4.7 %all-to-all-start.3 = ((bf16[16,64,128]{2,1,0:T(8,128)(2,1)}), bf16[16,64,128]{2,1,0:T(8,128)(2,1)S(1)}, u32[]{:S(2)}, u32[]{:S(2)}) async-start(bf16[16,64,128]{2,1,0:T(8,128)(2,1)} %shard_map.189), calls=%async_computation.3 | async-start | bytes 524288 | tf_op jit(solution)/shard_map/all_to_all | solution.py:306
  99.6 2.9 %shard_map.187.given_ref = bf16[2,256,2048]{2,1,0:T(8,128)(2,1)} custom-call(bf16[16,24,2048]{2,1,0:T(8,128)(2,1)} %all-to-all-done.1.rows_ref), custom_call_target="tpu_custom_call" | custom-call | tf_op jit(solution)/shard_map/pallas_call | solution.py:396
  102.5 8.8 %shard_map.188 = bf16[16,24,2048]{2,1,0:T(8,128)(2,1)} custom-call(bf16[2,256,2048]{2,1,0:T(8,128)(2,1)} %shard_map.187.given_ref, bf16[16,3,2,32,2048]{4,3,2,1,0:T(8,128)(2,1)} %bitcast.38, bf16[16,3,2,32,2048]{4,3,2,1,0:T(8,128)(2,1)} %bitcast.39), custom_call_target="tpu_custom_call" | custom-call | tf_op jit(solution)/shard_map/pallas_call | solution.py:398
  111.4 4.4 %all-to-all-start.4 = ((bf16[16,24,2048]{2,1,0:T(8,128)(2,1)}), bf16[16,24,2048]{2,1,0:T(8,128)(2,1)}, u32[]{:S(2)}, u32[]{:S(2)}) async-start(bf16[16,24,2048]{2,1,0:T(8,128)(2,1)} %shard_map.188), calls=%async_computation.4 | async-start | bytes 3145728 | tf_op jit(solution)/shard_map/all_to_all | solution.py:306
  116.4 2.8 %collective-permute-start.6 = (bf16[4,1024,128]{2,1,0:T(8,128)(2,1)}, bf16[4,1024,128]{2,1,0:T(8,128)(2,1)}, u32[]{:S(2)}, u32[]{:S(2)}) collective-permute-start(bf16[4,1024,128]{2,1,0:T(8,128)(2,1)} %collective-permute-done.4.refs_1_), channel_id=1, source_target_pairs={{0,64},{64,128},{128,192},{192,0},{65,1},{129,65},{193,129},{1,193... | collective-permute-start | bytes 3145736 | tf_op jit(solution)/shard_map/ppermute | solution.py:318
  119.2 1.8 %shard_map.191.tables_ref = bf16[2,128,384]{2,1,0:T(8,128)(2,1)} custom-call(s32[2,128]{1,0:T(2,128)} %bitcast.58, f32[2,128]{1,0:T(2,128)} %bitcast.59), custom_call_target="tpu_custom_call" | custom-call | tf_op jit(solution)/shard_map/pallas_call | solution.py:397
  121.0 0.6 pad_add_fusion.place_ref
  121.6 2.2 %fusion.10 = f32[128,512]{1,0:T(8,128)S(1)} fusion(bf16[128,2048]{1,0:T(8,128)(2,1)} %get-tuple-element.23, bf16[2048,512]{1,0:T(8,128)(2,1)} %param.33), kind=kOutput, calls=%fused_computation.18 | convolution fusion | flops 268435456 | bytes 2883584 | tf_op jit(solution)/shard_map/dot_general | solution.py:390
  123.9 3.4 %fusion.1.shared_ref = f32[128,2048]{1,0:T(8,128)} fusion(bf16[512,2048]{1,0:T(8,128)(2,1)S(1)} %copy-done, bf16[128,2048]{1,0:T(8,128)(2,1)S(1)} %copy-done.2, bf16[2048,512]{1,0:T(8,128)(2,1)} %param.34, f32[128,512]{1,0:T(8,128)S(1)} %fusion.10), kind=kOutput, calls=%fused_computation.2 | convolution fusion | flops 537264128 | bytes 6029312 | tf_op jit(solution)/shard_map/dot_general | solution.py:393
  127.3 19.5 %collective-permute-done.6.refs_3_ = bf16[4,1024,128]{2,1,0:T(8,128)(2,1)} collective-permute-done((bf16[4,1024,128]{2,1,0:T(8,128)(2,1)}, bf16[4,1024,128]{2,1,0:T(8,128)(2,1)}, u32[]{:S(2)}, u32[]{:S(2)}) %collective-permute-start.6) | collective-permute-done | bytes 1048608 | tf_op jit(solution)/shard_map/ppermute | solution.py:318
  146.8 4.4 %shard_map.190 = bf16[128,2048]{1,0:T(8,128)(2,1)} custom-call(s32[3]{0:T(128)} %pad_add_fusion.place_ref, bf16[8,2,64,128]{3,2,1,0:T(8,128)(2,1)} %bitcast.41, bf16[4,1024,128]{2,1,0:T(8,128)(2,1)} %copy-done.1, bf16[4,1024,128]{2,1,0:T(8,128)(2,1)} %collective-permute-done.4.refs_1_, bf16[4,1024,128]{2,1,0:T(8,128)(2,1)} %collective-permute-done.5.refs_2_, ...), custom_call_target="tpu_custom_call" | custom-call | tf_op jit(solution)/shard_map/pallas_call | solution.py:422
  151.1 3.3 %shard_map.192 = bf16[128,2048]{1,0:T(8,128)(2,1)} custom-call(bf16[2,128,384]{2,1,0:T(8,128)(2,1)} %shard_map.191.tables_ref, bf16[384,2048]{1,0:T(8,128)(2,1)} %bitcast.28.results_ref, f32[128,2048]{1,0:T(8,128)} %fusion.1.shared_ref), custom_call_target="tpu_custom_call" | custom-call | tf_op jit(solution)/shard_map/pallas_call | solution.py:417
  (27 shorter events, 1.3 us)
Async XLA Ops:
  7.2 116.7 %copy-start = (bf16[512,2048]{1,0:T(8,128)(2,1)S(1)}, bf16[512,2048]{1,0:T(8,128)(2,1)}, u32[]{:S(2)}) copy-start(bf16[512,2048]{1,0:T(8,128)(2,1)} %param.35) | copy-start | bytes 6291460
  7.2 95.3 %all-gather.3.cloned.1.call-start = ((), (), s32[]{:S(2)}) async-start(), calls=%async_computation.5 | async-start | bytes 13369344 | tf_op jit(solution)/shard_map/all_gather | solution.py:357
  10.9 16.8 %all-to-all-start = ((bf16[8,64,128]{2,1,0:T(8,128)(2,1)}), bf16[8,64,128]{2,1,0:T(8,128)(2,1)S(1)}, u32[]{:S(2)}, u32[]{:S(2)}) async-start(bf16[8,64,128]{2,1,0:T(8,128)(2,1)} %broadcast_in_dim.6), calls=%async_computation | async-start | bytes 262144 | tf_op jit(solution)/shard_map/all_to_all | solution.py:306
  27.7 45.1 %all-to-all-start.1 = ((bf16[16,24,2048]{2,1,0:T(8,128)(2,1)}), bf16[16,24,2048]{2,1,0:T(8,128)(2,1)}, u32[]{:S(2)}, u32[]{:S(2)}) async-start(bf16[16,24,2048]{2,1,0:T(8,128)(2,1)} %bitcast.40), calls=%async_computation.1 | async-start | bytes 3145728 | tf_op jit(solution)/shard_map/all_to_all | solution.py:306
  34.5 3.9 %collective-permute-start = (bf16[512,128]{1,0:T(8,128)(2,1)S(1)}, bf16[512,128]{1,0:T(8,128)(2,1)S(1)}, u32[]{:S(2)}, u32[]{:S(2)}) collective-permute-start(bf16[512,128]{1,0:T(8,128)(2,1)S(1)} %bitcast.42), channel_id=1, source_target_pairs={{0,1},{1,0},{2,3},{3,2},{4,5},{5,4},{6,7},{7,6},{8,9},{9,8},{10,11... | collective-permute-start | bytes 393224 | tf_op jit(solution)/shard_map/ppermute | solution.py:310
  38.4 18.5 %collective-permute-start.1 = (bf16[1024,128]{1,0:T(8,128)(2,1)S(1)}, bf16[1024,128]{1,0:T(8,128)(2,1)S(1)}, u32[]{:S(2)}, u32[]{:S(2)}) collective-permute-start(bf16[1024,128]{1,0:T(8,128)(2,1)S(1)} %get-tuple-element.25), channel_id=1, source_target_pairs={{0,16},{16,32},{32,48},{48,0},{17,1},{33,17},{49,33},{1,49},{2,18}... | collective-permute-start | bytes 786440 | tf_op jit(solution)/shard_map/ppermute | solution.py:316
  56.9 24.3 %copy-start.4 = (bf16[1024,128]{1,0:T(8,128)(2,1)}, bf16[1024,128]{1,0:T(8,128)(2,1)S(1)}, u32[]{:S(2)}) copy-start(bf16[1024,128]{1,0:T(8,128)(2,1)S(1)} %collective-permute-done.1) | copy-start | bytes 786436
  56.9 24.3 %collective-permute-start.3 = (bf16[1024,128]{1,0:T(8,128)(2,1)S(1)}, bf16[1024,128]{1,0:T(8,128)(2,1)S(1)}, u32[]{:S(2)}, u32[]{:S(2)}) collective-permute-start(bf16[1024,128]{1,0:T(8,128)(2,1)S(1)} %collective-permute-done.1), channel_id=1, source_target_pairs={{0,16},{16,32},{32,48},{48,0},{17,1},{33,17},{49,33},{1,49},{2,18}... | collective-permute-start | bytes 786440 | tf_op jit(solution)/shard_map/ppermute | solution.py:318
  57.3 23.8 %collective-permute-start.2 = (bf16[1024,128]{1,0:T(8,128)(2,1)S(1)}, bf16[1024,128]{1,0:T(8,128)(2,1)S(1)}, u32[]{:S(2)}, u32[]{:S(2)}) collective-permute-start(bf16[1024,128]{1,0:T(8,128)(2,1)S(1)} %collective-permute-done.1), channel_id=1, source_target_pairs={{0,1},{1,0},{2,3},{3,2},{4,5},{5,4},{6,7},{7,6},{8,9},{9,8},{10,11... | collective-permute-start | bytes 786440 | tf_op jit(solution)/shard_map/ppermute | solution.py:310
  74.3 17.9 %all-to-all-start.2 = ((f32[16,64,128]{2,1,0:T(8,128)}), f32[16,64,128]{2,1,0:T(8,128)}, u32[]{:S(2)}, u32[]{:S(2)}) async-start(f32[16,64,128]{2,1,0:T(8,128)} %broadcast_in_dim.7), calls=%async_computation.2 | async-start | bytes 1048576 | tf_op jit(solution)/shard_map/all_to_all | solution.py:306
  81.1 0.7 copy-start.5
  81.2 0.8 copy-start.6
  83.2 19.3 %copy-start.1 = (bf16[4,1024,128]{2,1,0:T(8,128)(2,1)}, bf16[4,1024,128]{2,1,0:T(8,128)(2,1)S(1)}, u32[]{:S(2)}) copy-start(bf16[4,1024,128]{2,1,0:T(8,128)(2,1)S(1)} %pad_maximum_fusion.refs_0_) | copy-start | bytes 3145732
  83.2 32.6 %collective-permute-start.4 = (bf16[4,1024,128]{2,1,0:T(8,128)(2,1)S(1)}, bf16[4,1024,128]{2,1,0:T(8,128)(2,1)}, u32[]{:S(2)}, u32[]{:S(2)}) collective-permute-start(bf16[4,1024,128]{2,1,0:T(8,128)(2,1)S(1)} %pad_maximum_fusion.refs_0_), channel_id=1, source_target_pairs={{0,64},{64,128},{128,192},{192,0},{65,1},{129,65},{193,129},{1,193... | collective-permute-start | bytes 3145736 | tf_op jit(solution)/shard_map/ppermute | solution.py:316
  94.9 16.5 %all-to-all-start.3 = ((bf16[16,64,128]{2,1,0:T(8,128)(2,1)}), bf16[16,64,128]{2,1,0:T(8,128)(2,1)S(1)}, u32[]{:S(2)}, u32[]{:S(2)}) async-start(bf16[16,64,128]{2,1,0:T(8,128)(2,1)} %shard_map.189), calls=%async_computation.3 | async-start | bytes 524288 | tf_op jit(solution)/shard_map/all_to_all | solution.py:306
  111.4 12.5 %copy-start.3 = (bf16[16,64,128]{2,1,0:T(8,128)(2,1)}, bf16[16,64,128]{2,1,0:T(8,128)(2,1)S(1)}, u32[]{:S(2)}) copy-start(bf16[16,64,128]{2,1,0:T(8,128)(2,1)S(1)} %all-to-all-done.3) | copy-start | bytes 786436
  111.4 39.8 %all-to-all-start.4 = ((bf16[16,24,2048]{2,1,0:T(8,128)(2,1)}), bf16[16,24,2048]{2,1,0:T(8,128)(2,1)}, u32[]{:S(2)}, u32[]{:S(2)}) async-start(bf16[16,24,2048]{2,1,0:T(8,128)(2,1)} %shard_map.188), calls=%async_computation.4 | async-start | bytes 3145728 | tf_op jit(solution)/shard_map/all_to_all | solution.py:306
  115.8 8.1 %copy-start.2 = (bf16[128,2048]{1,0:T(8,128)(2,1)S(1)}, bf16[128,2048]{1,0:T(8,128)(2,1)}, u32[]{:S(2)}) copy-start(bf16[128,2048]{1,0:T(8,128)(2,1)} %get-tuple-element.23) | copy-start | bytes 1572868
  115.8 11.5 %collective-permute-start.5 = (bf16[4,1024,128]{2,1,0:T(8,128)(2,1)}, bf16[4,1024,128]{2,1,0:T(8,128)(2,1)}, u32[]{:S(2)}, u32[]{:S(2)}) collective-permute-start(bf16[4,1024,128]{2,1,0:T(8,128)(2,1)} %collective-permute-done.4.refs_1_), channel_id=1, source_target_pairs={{0,1},{1,0},{2,3},{3,2},{4,5},{5,4},{6,7},{7,6},{8,9},{9,8},{10,11... | collective-permute-start | bytes 3145736 | tf_op jit(solution)/shard_map/ppermute | solution.py:310
  116.4 30.4 %collective-permute-start.6 = (bf16[4,1024,128]{2,1,0:T(8,128)(2,1)}, bf16[4,1024,128]{2,1,0:T(8,128)(2,1)}, u32[]{:S(2)}, u32[]{:S(2)}) collective-permute-start(bf16[4,1024,128]{2,1,0:T(8,128)(2,1)} %collective-permute-done.4.refs_1_), channel_id=1, source_target_pairs={{0,64},{64,128},{128,192},{192,0},{65,1},{129,65},{193,129},{1,193... | collective-permute-start | bytes 3145736 | tf_op jit(solution)/shard_map/ppermute | solution.py:318
Sparse Core Ops, SparseCore 0:
  9.8 79.9 all-gather.2

commit v4 on v3

--- a/solution.py
+++ b/solution.py
@@ -205,6 +205,17 @@
     sent_ref[...] = mm(filled.astype(F32), normed).astype(BF)
 
 
+def pack_kernel(first_ref, second_ref, third_ref, out_ref, sems):
+    copies = [
+        pltpu.make_async_copy(ref, out_ref.at[k], sems.at[k])
+        for k, ref in enumerate((first_ref, second_ref, third_ref))
+    ]
+    for copy in copies:
+        copy.start()
+    for copy in copies:
+        copy.wait()
+
+
 def regroup_kernel(rows_ref, out_ref):
     rows, width = out_ref.shape[1] // 2, out_ref.shape[2]
     both = rows_ref[:, 16:24].reshape(rows, width)
@@ -270,9 +281,12 @@
 
 
 def combine_kernel(tables_ref, results_ref, shared_ref, out_ref):
-    results = results_ref[...]
-    out = shared_ref[...] + (mm(tables_ref[0], results) + mm(tables_ref[1], results))
-    out_ref[...] = out.astype(BF)
+    step = 512
+    for k in range(0, out_ref.shape[1], step):
+        at = slice(k, k + step)
+        results = results_ref[:, at]
+        out = shared_ref[:, at] + (mm(tables_ref[0], results) + mm(tables_ref[1], results))
+        out_ref[:, at] = out.astype(BF)
 
 
 def project_kernel(place_ref, rows_ref, *refs):
@@ -353,7 +367,15 @@
     length, dim = key_in.shape
     tokens, width = moe_in.shape
 
-    local_weights = jnp.stack([w.transpose(0, 2, 1) for w in (expert_gate, expert_up, expert_down)])
+    weights = [w.transpose(0, 2, 1) for w in (expert_gate, expert_up, expert_down)]
+    hbm = pl.BlockSpec(memory_space=pl.ANY)
+    local_weights = call(
+        pack_kernel,
+        shape((3, *weights[0].shape), BF),
+        in_specs=[hbm] * 3,
+        out_specs=hbm,
+        scratch_shapes=[pltpu.SemaphoreType.DMA((3,))],
+    )(*weights)
     all_weights = lax.all_gather(local_weights, TP)
 
     core = lax.axis_index("core")

time: 162 us -> 185 us (1.14)
  Pallas kernels: 41.2 us -> 66.1 us
  other arithmetic: 4.16 us -> 1.91 us
    pallas_call x0 -> x1, Pallas kernels: none -> 25 us  [shards(): call(pack_kernel, shape((3, *weights[0].shape), BF), in_specs=[hbm] * 3,...]
    another operation x1 -> x0, other arithmetic: 2.25 us -> none  [shards(): jnp.stack([w.transpose(0, 2, 1) for w in (expert_gate, expert_up, expert_...]
  transfers between devices with their start and end apart: 13 -> 13, of which waited for: 5 -> 5; matrix products, arithmetic and copies ran while one was open for 7% -> 6% of each run, Pallas kernels for 23% -> 21%
where the time goes in v4:
time: 185 us; the launch traced here: 184 us
  Pallas kernels  66.1 us (36%)
  waiting for transfers between devices  47.4 us (26%)
  starting transfers between devices  44.9 us (24%)
  between operations  14.2 us (8%)
  matrix products  5.61 us (3%)
  local copies, waits for them, and re-layouts  3.78 us (2%)
  other arithmetic  1.91 us (1%)
    all_to_all x5, starting transfers between devices, swap(): return lax.all_to_all(array, axes, split_axis=0, concat_axis=0, tiled=True)  31.8 us
    pallas_call x1, Pallas kernels, shards(): call(pack_kernel, shape((3, *weights[0].shape), BF), in_specs=[hbm] * 3,...  25 us
    ppermute x2, waiting for transfers between devices, around(): last = lax.ppermute(came, (axis, 'core'), pairs)  19.5 us
    ppermute x2, waiting for transfers between devices, around(): came = lax.ppermute(block, (axis, 'core'), pairs)  15.7 us
    pallas_call x1, Pallas kernels, shards(): call(scan_kernel, (shape((2 * dim, length), F32), shape((dim, 2 * dim), F...  14.2 us
    all_to_all x5, waiting for transfers between devices, swap(): return lax.all_to_all(array, axes, split_axis=0, concat_axis=0, tiled=True)  11 us
    pallas_call x1, Pallas kernels, shards(): call(expert_kernel, shape((groups, slots, width), BF), grid=(2, 2), in_sp...  8.84 us
    ppermute x2, starting transfers between devices, around(): came = lax.ppermute(block, (axis, 'core'), pairs)  5.27 us
  transfers between devices with their start and end apart: 13, of which 5 were waited for; matrix products, arithmetic and copies ran while one was open for 6% of the time, Pallas kernels for 21%

profile of v4, /device:TPU:1, one launch (start us, length us, event | category | flops | bytes accessed | tf_op | source)
XLA Modules:
  0.0 183.9 jit_solution(10294921367328323978)
XLA Ops:
  7.2 25.0 %shard_map.188 = bf16[3,2,32,2048]{3,2,1,0:T(8,128)(2,1)} custom-call(bf16[2,32,2048]{2,1,0:T(8,128)(2,1)} %bitcast.43, bf16[2,32,2048]{2,1,0:T(8,128)(2,1)} %bitcast.44, bf16[2,32,2048]{2,1,0:T(8,128)(2,1)} %bitcast.45), custom_call_target="tpu_custom_call" | custom-call | tf_op jit(solution)/shard_map/pallas_call | solution.py:372
  32.2 0.7 constant_dynamic-slice_fusion
  32.9 0.7 broadcast_in_dim.6
  33.6 9.0 %all-to-all-start = ((bf16[8,64,128]{2,1,0:T(8,128)(2,1)}), bf16[8,64,128]{2,1,0:T(8,128)(2,1)S(1)}, u32[]{:S(2)}, u32[]{:S(2)}) async-start(bf16[8,64,128]{2,1,0:T(8,128)(2,1)} %broadcast_in_dim.6), calls=%async_computation | async-start | bytes 262144 | tf_op jit(solution)/shard_map/all_to_all | solution.py:320
  42.6 3.2 %shard_map.185 = (bf16[128,2048]{1,0:T(8,128)(2,1)}, bf16[384,2048]{1,0:T(8,128)(2,1)}) custom-call(bf16[128,2048]{1,0:T(8,128)(2,1)} %moe_ref.1, f32[1,2048]{1,0:T(1,128)} %bitcast.50, s32[2,128]{1,0:T(2,128)} %bitcast.51), custom_call_target="tpu_custom_call" | custom-call | tf_op jit(solution)/shard_map/pallas_call | solution.py:384
  45.8 4.6 %all-to-all-done = bf16[8,64,128]{2,1,0:T(8,128)(2,1)S(1)} async-done(((bf16[8,64,128]{2,1,0:T(8,128)(2,1)}), bf16[8,64,128]{2,1,0:T(8,128)(2,1)S(1)}, u32[]{:S(2)}, u32[]{:S(2)}) %all-to-all-start) | async-done | bytes 131104 | tf_op jit(solution)/shard_map/all_to_all | solution.py:320
  50.4 6.8 %all-to-all-start.1 = ((bf16[16,24,2048]{2,1,0:T(8,128)(2,1)}), bf16[16,24,2048]{2,1,0:T(8,128)(2,1)}, u32[]{:S(2)}, u32[]{:S(2)}) async-start(bf16[16,24,2048]{2,1,0:T(8,128)(2,1)} %bitcast.34), calls=%async_computation.1 | async-start | bytes 3145728 | tf_op jit(solution)/shard_map/all_to_all | solution.py:320
  57.2 2.8 %collective-permute-start = (bf16[512,128]{1,0:T(8,128)(2,1)S(1)}, bf16[512,128]{1,0:T(8,128)(2,1)S(1)}, u32[]{:S(2)}, u32[]{:S(2)}) collective-permute-start(bf16[512,128]{1,0:T(8,128)(2,1)S(1)} %bitcast.36), channel_id=1, source_target_pairs={{0,1},{1,0},{2,3},{3,2},{4,5},{5,4},{6,7},{7,6},{8,9},{9,8},{10,11... | collective-permute-start | bytes 393224 | tf_op jit(solution)/shard_map/ppermute | solution.py:324
  60.0 1.1 collective-permute-done
  61.2 2.7 %collective-permute-start.1 = (bf16[1024,128]{1,0:T(8,128)(2,1)S(1)}, bf16[1024,128]{1,0:T(8,128)(2,1)S(1)}, u32[]{:S(2)}, u32[]{:S(2)}) collective-permute-start(bf16[1024,128]{1,0:T(8,128)(2,1)S(1)} %get-tuple-element.25), channel_id=1, source_target_pairs={{0,16},{16,32},{32,48},{48,0},{17,1},{33,17},{49,33},{1,49},{2,18}... | collective-permute-start | bytes 786440 | tf_op jit(solution)/shard_map/ppermute | solution.py:330
  63.8 15.7 %collective-permute-done.1 = bf16[1024,128]{1,0:T(8,128)(2,1)S(1)} collective-permute-done((bf16[1024,128]{1,0:T(8,128)(2,1)S(1)}, bf16[1024,128]{1,0:T(8,128)(2,1)S(1)}, u32[]{:S(2)}, u32[]{:S(2)}) %collective-permute-start.1) | collective-permute-done | bytes 262176 | tf_op jit(solution)/shard_map/ppermute | solution.py:330
  80.0 1.2 collective-permute-start.2
  81.2 14.2 %shard_map.186 = (f32[128,2048]{1,0:T(8,128)}, f32[64,128]{1,0:T(8,128)}) custom-call(bf16[64,2048]{1,0:T(8,128)(2,1)} %bitcast.38, bf16[64,2048]{1,0:T(8,128)(2,1)} %bitcast.39, bf16[64,2048]{1,0:T(8,128)(2,1)} %bitcast.40, bf16[64,2048]{1,0:T(8,128)(2,1)} %bitcast.41, bf16[64,2048]{1,0:T(8,128)(2,1)} %bitcast.42), custom_call_target="tpu_custom_call" | custom-call | tf_op jit(solution)/shard_map/pallas_call | solution.py:398
  95.4 1.6 broadcast_in_dim.7
  97.0 6.8 %all-to-all-start.2 = ((f32[16,64,128]{2,1,0:T(8,128)}), f32[16,64,128]{2,1,0:T(8,128)}, u32[]{:S(2)}, u32[]{:S(2)}) async-start(f32[16,64,128]{2,1,0:T(8,128)} %broadcast_in_dim.7), calls=%async_computation.2 | async-start | bytes 1048576 | tf_op jit(solution)/shard_map/all_to_all | solution.py:320
  103.9 0.7 copy-done.5
  104.6 1.2 pad_maximum_fusion.refs_0_
  105.9 2.6 %collective-permute-start.4 = (bf16[4,1024,128]{2,1,0:T(8,128)(2,1)S(1)}, bf16[4,1024,128]{2,1,0:T(8,128)(2,1)}, u32[]{:S(2)}, u32[]{:S(2)}) collective-permute-start(bf16[4,1024,128]{2,1,0:T(8,128)(2,1)S(1)} %pad_maximum_fusion.refs_0_), channel_id=1, source_target_pairs={{0,64},{64,128},{128,192},{192,0},{65,1},{129,65},{193,129},{1,193... | collective-permute-start | bytes 3145736 | tf_op jit(solution)/shard_map/ppermute | solution.py:330
  108.5 6.4 %all-to-all-done.2.totals_ref = f32[16,64,128]{2,1,0:T(8,128)} async-done(((f32[16,64,128]{2,1,0:T(8,128)}), f32[16,64,128]{2,1,0:T(8,128)}, u32[]{:S(2)}, u32[]{:S(2)}) %all-to-all-start.2) | async-done | bytes 524320 | tf_op jit(solution)/shard_map/all_to_all | solution.py:320
  114.9 2.6 %shard_map.190 = bf16[16,64,128]{2,1,0:T(8,128)(2,1)} custom-call(s32[1]{0:T(128)} %bitcast.16.here_ref, f32[16,64,128]{2,1,0:T(8,128)} %all-to-all-done.2.totals_ref, f32[128,2048]{1,0:T(8,128)} %get-tuple-element.19.reads_ref, bf16[64,2048]{1,0:T(8,128)(2,1)} %bitcast.46, f32[1,64]{1,0:T(1,128)} %bitcast.54), custom_call_target="tpu_custom_call" | custom-call | tf_op jit(solution)/shard_map/pallas_call | solution.py:405
  117.5 4.8 %all-to-all-start.3 = ((bf16[16,64,128]{2,1,0:T(8,128)(2,1)}), bf16[16,64,128]{2,1,0:T(8,128)(2,1)S(1)}, u32[]{:S(2)}, u32[]{:S(2)}) async-start(bf16[16,64,128]{2,1,0:T(8,128)(2,1)} %shard_map.190), calls=%async_computation.3 | async-start | bytes 524288 | tf_op jit(solution)/shard_map/all_to_all | solution.py:320
  122.3 2.9 %shard_map.187.given_ref = bf16[2,256,2048]{2,1,0:T(8,128)(2,1)} custom-call(bf16[16,24,2048]{2,1,0:T(8,128)(2,1)} %all-to-all-done.1.rows_ref), custom_call_target="tpu_custom_call" | custom-call | tf_op jit(solution)/shard_map/pallas_call | solution.py:418
  125.2 8.8 %shard_map.189 = bf16[16,24,2048]{2,1,0:T(8,128)(2,1)} custom-call(bf16[2,256,2048]{2,1,0:T(8,128)(2,1)} %shard_map.187.given_ref, bf16[16,3,2,32,2048]{4,3,2,1,0:T(8,128)(2,1)} %bitcast.32, bf16[16,3,2,32,2048]{4,3,2,1,0:T(8,128)(2,1)} %bitcast.33), custom_call_target="tpu_custom_call" | custom-call | tf_op jit(solution)/shard_map/pallas_call | solution.py:420
  134.0 4.4 %all-to-all-start.4 = ((bf16[16,24,2048]{2,1,0:T(8,128)(2,1)}), bf16[16,24,2048]{2,1,0:T(8,128)(2,1)}, u32[]{:S(2)}, u32[]{:S(2)}) async-start(bf16[16,24,2048]{2,1,0:T(8,128)(2,1)} %shard_map.189), calls=%async_computation.4 | async-start | bytes 3145728 | tf_op jit(solution)/shard_map/all_to_all | solution.py:320
  139.1 2.8 %collective-permute-start.6 = (bf16[4,1024,128]{2,1,0:T(8,128)(2,1)}, bf16[4,1024,128]{2,1,0:T(8,128)(2,1)}, u32[]{:S(2)}, u32[]{:S(2)}) collective-permute-start(bf16[4,1024,128]{2,1,0:T(8,128)(2,1)} %collective-permute-done.4.refs_1_), channel_id=1, source_target_pairs={{0,64},{64,128},{128,192},{192,0},{65,1},{129,65},{193,129},{1,193... | collective-permute-start | bytes 3145736 | tf_op jit(solution)/shard_map/ppermute | solution.py:332
  141.9 1.8 shard_map.192.tables_ref
  143.7 0.6 pad_add_fusion.place_ref
  144.3 2.2 %fusion.10 = f32[128,512]{1,0:T(8,128)S(1)} fusion(bf16[128,2048]{1,0:T(8,128)(2,1)} %get-tuple-element.23, bf16[2048,512]{1,0:T(8,128)(2,1)} %param.33), kind=kOutput, calls=%fused_computation.17 | convolution fusion | flops 268435456 | bytes 2883584 | tf_op jit(solution)/shard_map/dot_general | solution.py:412
  146.6 3.4 %fusion.1.shared_ref = f32[128,2048]{1,0:T(8,128)} fusion(bf16[512,2048]{1,0:T(8,128)(2,1)S(1)} %copy-done, bf16[128,2048]{1,0:T(8,128)(2,1)S(1)} %copy-done.2, bf16[2048,512]{1,0:T(8,128)(2,1)} %param.34, f32[128,512]{1,0:T(8,128)S(1)} %fusion.10), kind=kOutput, calls=%fused_computation.2 | convolution fusion | flops 537264128 | bytes 6029312 | tf_op jit(solution)/shard_map/dot_general | solution.py:415
  150.0 19.5 %collective-permute-done.6.refs_3_ = bf16[4,1024,128]{2,1,0:T(8,128)(2,1)} collective-permute-done((bf16[4,1024,128]{2,1,0:T(8,128)(2,1)}, bf16[4,1024,128]{2,1,0:T(8,128)(2,1)}, u32[]{:S(2)}, u32[]{:S(2)}) %collective-permute-start.6) | collective-permute-done | bytes 1048608 | tf_op jit(solution)/shard_map/ppermute | solution.py:332
  169.5 4.4 %shard_map.191 = bf16[128,2048]{1,0:T(8,128)(2,1)} custom-call(s32[3]{0:T(128)} %pad_add_fusion.place_ref, bf16[8,2,64,128]{3,2,1,0:T(8,128)(2,1)} %bitcast.35, bf16[4,1024,128]{2,1,0:T(8,128)(2,1)} %copy-done.1, bf16[4,1024,128]{2,1,0:T(8,128)(2,1)} %collective-permute-done.4.refs_1_, bf16[4,1024,128]{2,1,0:T(8,128)(2,1)} %collective-permute-done.5.refs_2_, ...), custom_call_target="tpu_custom_call" | custom-call | tf_op jit(solution)/shard_map/pallas_call | solution.py:444
  173.8 3.3 %shard_map.193 = bf16[128,2048]{1,0:T(8,128)(2,1)} custom-call(bf16[2,128,384]{2,1,0:T(8,128)(2,1)} %shard_map.192.tables_ref, bf16[384,2048]{1,0:T(8,128)(2,1)} %bitcast.25.results_ref, f32[128,2048]{1,0:T(8,128)} %fusion.1.shared_ref), custom_call_target="tpu_custom_call" | custom-call | tf_op jit(solution)/shard_map/pallas_call | solution.py:439
  (27 shorter events, 1.3 us)
Async XLA Ops:
  7.2 139.4 %copy-start = (bf16[512,2048]{1,0:T(8,128)(2,1)S(1)}, bf16[512,2048]{1,0:T(8,128)(2,1)}, u32[]{:S(2)}) copy-start(bf16[512,2048]{1,0:T(8,128)(2,1)} %param.35) | copy-start | bytes 6291460
  7.2 118.0 %all-gather.3.cloned.1.call-start = ((), (), s32[]{:S(2)}) async-start(), calls=%async_computation.5 | async-start | bytes 13369344 | tf_op jit(solution)/shard_map/all_gather | solution.py:379
  33.6 16.8 %all-to-all-start = ((bf16[8,64,128]{2,1,0:T(8,128)(2,1)}), bf16[8,64,128]{2,1,0:T(8,128)(2,1)S(1)}, u32[]{:S(2)}, u32[]{:S(2)}) async-start(bf16[8,64,128]{2,1,0:T(8,128)(2,1)} %broadcast_in_dim.6), calls=%async_computation | async-start | bytes 262144 | tf_op jit(solution)/shard_map/all_to_all | solution.py:320
  50.4 45.0 %all-to-all-start.1 = ((bf16[16,24,2048]{2,1,0:T(8,128)(2,1)}), bf16[16,24,2048]{2,1,0:T(8,128)(2,1)}, u32[]{:S(2)}, u32[]{:S(2)}) async-start(bf16[16,24,2048]{2,1,0:T(8,128)(2,1)} %bitcast.34), calls=%async_computation.1 | async-start | bytes 3145728 | tf_op jit(solution)/shard_map/all_to_all | solution.py:320
  57.2 3.9 %collective-permute-start = (bf16[512,128]{1,0:T(8,128)(2,1)S(1)}, bf16[512,128]{1,0:T(8,128)(2,1)S(1)}, u32[]{:S(2)}, u32[]{:S(2)}) collective-permute-start(bf16[512,128]{1,0:T(8,128)(2,1)S(1)} %bitcast.36), channel_id=1, source_target_pairs={{0,1},{1,0},{2,3},{3,2},{4,5},{5,4},{6,7},{7,6},{8,9},{9,8},{10,11... | collective-permute-start | bytes 393224 | tf_op jit(solution)/shard_map/ppermute | solution.py:324
  61.2 18.4 %collective-permute-start.1 = (bf16[1024,128]{1,0:T(8,128)(2,1)S(1)}, bf16[1024,128]{1,0:T(8,128)(2,1)S(1)}, u32[]{:S(2)}, u32[]{:S(2)}) collective-permute-start(bf16[1024,128]{1,0:T(8,128)(2,1)S(1)} %get-tuple-element.25), channel_id=1, source_target_pairs={{0,16},{16,32},{32,48},{48,0},{17,1},{33,17},{49,33},{1,49},{2,18}... | collective-permute-start | bytes 786440 | tf_op jit(solution)/shard_map/ppermute | solution.py:330
  79.6 24.3 %copy-start.4 = (bf16[1024,128]{1,0:T(8,128)(2,1)}, bf16[1024,128]{1,0:T(8,128)(2,1)S(1)}, u32[]{:S(2)}) copy-start(bf16[1024,128]{1,0:T(8,128)(2,1)S(1)} %collective-permute-done.1) | copy-start | bytes 786436
  79.6 24.3 %collective-permute-start.3 = (bf16[1024,128]{1,0:T(8,128)(2,1)S(1)}, bf16[1024,128]{1,0:T(8,128)(2,1)S(1)}, u32[]{:S(2)}, u32[]{:S(2)}) collective-permute-start(bf16[1024,128]{1,0:T(8,128)(2,1)S(1)} %collective-permute-done.1), channel_id=1, source_target_pairs={{0,16},{16,32},{32,48},{48,0},{17,1},{33,17},{49,33},{1,49},{2,18}... | collective-permute-start | bytes 786440 | tf_op jit(solution)/shard_map/ppermute | solution.py:332
  80.0 23.8 %collective-permute-start.2 = (bf16[1024,128]{1,0:T(8,128)(2,1)S(1)}, bf16[1024,128]{1,0:T(8,128)(2,1)S(1)}, u32[]{:S(2)}, u32[]{:S(2)}) collective-permute-start(bf16[1024,128]{1,0:T(8,128)(2,1)S(1)} %collective-permute-done.1), channel_id=1, source_target_pairs={{0,1},{1,0},{2,3},{3,2},{4,5},{5,4},{6,7},{7,6},{8,9},{9,8},{10,11... | collective-permute-start | bytes 786440 | tf_op jit(solution)/shard_map/ppermute | solution.py:324
  97.0 17.9 %all-to-all-start.2 = ((f32[16,64,128]{2,1,0:T(8,128)}), f32[16,64,128]{2,1,0:T(8,128)}, u32[]{:S(2)}, u32[]{:S(2)}) async-start(f32[16,64,128]{2,1,0:T(8,128)} %broadcast_in_dim.7), calls=%async_computation.2 | async-start | bytes 1048576 | tf_op jit(solution)/shard_map/all_to_all | solution.py:320
  103.8 0.7 copy-start.5
  103.8 0.8 copy-start.6
  105.9 19.3 %copy-start.1 = (bf16[4,1024,128]{2,1,0:T(8,128)(2,1)}, bf16[4,1024,128]{2,1,0:T(8,128)(2,1)S(1)}, u32[]{:S(2)}) copy-start(bf16[4,1024,128]{2,1,0:T(8,128)(2,1)S(1)} %pad_maximum_fusion.refs_0_) | copy-start | bytes 3145732
  105.9 32.6 %collective-permute-start.4 = (bf16[4,1024,128]{2,1,0:T(8,128)(2,1)S(1)}, bf16[4,1024,128]{2,1,0:T(8,128)(2,1)}, u32[]{:S(2)}, u32[]{:S(2)}) collective-permute-start(bf16[4,1024,128]{2,1,0:T(8,128)(2,1)S(1)} %pad_maximum_fusion.refs_0_), channel_id=1, source_target_pairs={{0,64},{64,128},{128,192},{192,0},{65,1},{129,65},{193,129},{1,193... | collective-permute-start | bytes 3145736 | tf_op jit(solution)/shard_map/ppermute | solution.py:330
  117.5 16.5 %all-to-all-start.3 = ((bf16[16,64,128]{2,1,0:T(8,128)(2,1)}), bf16[16,64,128]{2,1,0:T(8,128)(2,1)S(1)}, u32[]{:S(2)}, u32[]{:S(2)}) async-start(bf16[16,64,128]{2,1,0:T(8,128)(2,1)} %shard_map.190), calls=%async_computation.3 | async-start | bytes 524288 | tf_op jit(solution)/shard_map/all_to_all | solution.py:320
  134.0 12.5 %copy-start.3 = (bf16[16,64,128]{2,1,0:T(8,128)(2,1)}, bf16[16,64,128]{2,1,0:T(8,128)(2,1)S(1)}, u32[]{:S(2)}) copy-start(bf16[16,64,128]{2,1,0:T(8,128)(2,1)S(1)} %all-to-all-done.3) | copy-start | bytes 786436
  134.0 39.8 %all-to-all-start.4 = ((bf16[16,24,2048]{2,1,0:T(8,128)(2,1)}), bf16[16,24,2048]{2,1,0:T(8,128)(2,1)}, u32[]{:S(2)}, u32[]{:S(2)}) async-start(bf16[16,24,2048]{2,1,0:T(8,128)(2,1)} %shard_map.189), calls=%async_computation.4 | async-start | bytes 3145728 | tf_op jit(solution)/shard_map/all_to_all | solution.py:320
  138.5 8.1 %copy-start.2 = (bf16[128,2048]{1,0:T(8,128)(2,1)S(1)}, bf16[128,2048]{1,0:T(8,128)(2,1)}, u32[]{:S(2)}) copy-start(bf16[128,2048]{1,0:T(8,128)(2,1)} %get-tuple-element.23) | copy-start | bytes 1572868
  138.5 11.5 %collective-permute-start.5 = (bf16[4,1024,128]{2,1,0:T(8,128)(2,1)}, bf16[4,1024,128]{2,1,0:T(8,128)(2,1)}, u32[]{:S(2)}, u32[]{:S(2)}) collective-permute-start(bf16[4,1024,128]{2,1,0:T(8,128)(2,1)} %collective-permute-done.4.refs_1_), channel_id=1, source_target_pairs={{0,1},{1,0},{2,3},{3,2},{4,5},{5,4},{6,7},{7,6},{8,9},{9,8},{10,11... | collective-permute-start | bytes 3145736 | tf_op jit(solution)/shard_map/ppermute | solution.py:324
  139.1 30.4 %collective-permute-start.6 = (bf16[4,1024,128]{2,1,0:T(8,128)(2,1)}, bf16[4,1024,128]{2,1,0:T(8,128)(2,1)}, u32[]{:S(2)}, u32[]{:S(2)}) collective-permute-start(bf16[4,1024,128]{2,1,0:T(8,128)(2,1)} %collective-permute-done.4.refs_1_), channel_id=1, source_target_pairs={{0,64},{64,128},{128,192},{192,0},{65,1},{129,65},{193,129},{1,193... | collective-permute-start | bytes 3145736 | tf_op jit(solution)/shard_map/ppermute | solution.py:332
Sparse Core Ops, SparseCore 0:
  32.3 79.9 all-gather.2
